TPU v7x, 32 devices: a whole 2x2x4 slice. The times are simulated.
32 devices in a mesh: grp: 2 (over y), fs: 4 (over z), tp: 4 (over x, core).
Axes of the slice: x: 2, y: 2, z: 4, core: 2. Of those that a mesh axis runs over, the one named last changes fastest.
Arguments:
- tokens: bfloat16 [2048, 2048], P(('grp', 'fs')), parts along dimension 0, may hold values from -6 to 6
- ffn_pre_gain: bfloat16 [2048], replicated, may hold values from 0.099609375 to 1.8984375
- gate_weight: bfloat16 [2048, 5632], P('fs', 'tp'), may hold values from -0.125 to 0.125
- up_weight: bfloat16 [2048, 5632], P('fs', 'tp'), may hold values from -0.125 to 0.125
- down_weight: bfloat16 [5632, 2048], P('tp', 'fs'), may hold values from -0.078125 to 0.078125
- ffn_post_gain: bfloat16 [2048], replicated, may hold values from 0.099609375 to 1.8984375
- mix_pre_gain: bfloat16 [2048], replicated, may hold values from 0.099609375 to 1.8984375
- mix_u_weight: bfloat16 [2048, 2048], P('fs', 'tp'), may hold values from -0.125 to 0.125
- mix_v_weight: bfloat16 [2048, 2048], P('fs', 'tp'), may hold values from -0.125 to 0.125
- spatial_gain: bfloat16 [2048], P('tp'), may hold values from 0.099609375 to 1.8984375
- spatial_weight: bfloat16 [16, 128, 128], P('tp'), may hold values from -0.5 to 0.5
- spatial_bias: bfloat16 [16, 128], P('tp'), may hold values from 0.099609375 to 1.8984375
- mix_out_weight: bfloat16 [2048, 2048], P('tp', 'fs'), may hold values from -0.125 to 0.125
- mix_post_gain: bfloat16 [2048], replicated, may hold values from 0.099609375 to 1.8984375
- late_pre_gain: bfloat16 [2048], replicated, may hold values from 0.099609375 to 1.8984375
- late_post_gain: bfloat16 [2048], replicated, may hold values from 0.099609375 to 1.8984375
Outputs:
- result: bfloat16 [2048, 2048], P(('grp', 'fs')), parts along dimension 0
There are 2 independent parts, one for each index of `grp`. A program takes and returns all parts, laid end to end along the dimension named above; an argument that names none is the same for every part. Nothing has to cross between parts.
All inputs are finite; a program needn't handle non-finite values.
Results may differ from a plain program's by a relative error of at most 0.019.
Values may be sent and summed in bfloat16 or wider, within the bound.
A program may use at most 128 MiB of HBM per device.

v0:
```python
import functools
import math

import jax
import jax.numpy as jnp
from jax import lax
from jax.experimental import pallas as pl
from jax.experimental.pallas import tpu as pltpu
from jax.sharding import PartitionSpec as P

GROUP_WIDTH = 128
BLOCK = 128
TILE = 256
F32 = jnp.float32
BF16 = jnp.bfloat16
MESH = pl.DeviceIdType.MESH
SPLITS = (2, 2, 2, 1, 1, 2)
PIECE = 32


def aligned(value, unit):
    return value if isinstance(value, int) else pl.multiple_of(value, unit)


def over_tiles(width, body):
    count = width // TILE

    def step(i, carry):
        body(pl.multiple_of(i * TILE, TILE), TILE)
        return carry

    lax.fori_loop(0, count, step, 0)
    if width % TILE:
        body(count * TILE, width % TILE)


def over_rows(count, size, body):
    def step(i, carry):
        body(pl.multiple_of(i * size, size))
        return carry

    lax.fori_loop(0, count // size, step, 0)


def gelu(a):
    return 0.5 * a * (1.0 + lax.erf(a * (2.0**-0.5)))


def kernel(
    sizes,
    tokens,
    gain0,
    gain1,
    gain2,
    gain3,
    gain4,
    gain5,
    gate_w,
    up_w,
    down_w,
    u_w,
    v_w,
    out_w,
    spatial_gain,
    spatial_weight,
    spatial_bias,
    result,
    gate_full,
    up_full,
    down_full,
    u_full,
    v_full,
    out_full,
    normed,
    hidden,
    mixed,
    parts,
    paired,
    outgoing,
    landed,
    streams,
    own_sem,
    left_send,
    left_recv,
    right_send,
    right_recv,
    side_send,
    side_recv,
    pair_send,
    pair_recv,
    sum_send,
    sum_recv,
    twin_send,
    twin_recv,
    put_send,
    put_recv,
    pass_send,
    pass_recv,
    last_sem,
):
    grp_n, fs_n, tp_n = sizes
    grp, fs, tp = lax.axis_index("grp"), lax.axis_index("fs"), lax.axis_index("tp")
    shards = (gate_w, up_w, down_w, u_w, v_w, out_w)
    fulls = (gate_full, up_full, down_full, u_full, v_full, out_full)
    count, width = tokens.shape
    chunk = count // tp_n
    chips = tp_n // 2
    chip, core = tp // 2, lax.rem(tp, 2)
    twin = tp + 1 - 2 * core
    columns = pair_send.shape[1]
    column = width // columns
    piece_n = put_send.shape[1]
    piece_rows = chunk // piece_n
    all_gains = (gain0, gain1, gain2, gain3, gain4, gain5)

    barrier = pltpu.get_barrier_semaphore()
    for move in (1, fs_n - 1):
        pl.semaphore_signal(
            barrier, inc=1, device_id={"fs": lax.rem(fs + move, fs_n)}, device_id_type=MESH
        )
    for move in range(1, grp_n):
        pl.semaphore_signal(
            barrier, inc=1, device_id={"grp": lax.rem(grp + move, grp_n)}, device_id_type=MESH
        )
    for move in range(1, tp_n):
        pl.semaphore_signal(
            barrier, inc=1, device_id={"tp": lax.rem(tp + move, tp_n)}, device_id_type=MESH
        )
    pl.semaphore_wait(barrier, 2 + grp_n - 1 + tp_n - 1)

    units = []
    for w in range(6):
        piece = shards[w].shape[0] // grp_n // SPLITS[w]
        for s in range(SPLITS[w]):
            units.append((w, s * piece, piece))

    def unit_rows(unit):
        w, low, piece = units[unit]
        return aligned(grp * (shards[w].shape[0] // grp_n) + low, 16), piece

    def place(w, block, low, piece):
        if w in (2, 5):
            return fulls[w].at[block, pl.ds(low, piece), :]
        start = aligned(block * shards[w].shape[0] + low, 16)
        return fulls[w].at[pl.ds(start, piece), :]

    def own_copy(w):
        return pltpu.make_async_copy(
            shards[w], place(w, fs, 0, shards[w].shape[0]), own_sem.at[w]
        )

    def to_right(unit, hop, own=False):
        w = units[unit][0]
        low, piece = unit_rows(unit)
        target = place(w, fs - hop, low, piece)
        source = shards[w].at[pl.ds(low, piece), :] if own else target
        return pltpu.make_async_remote_copy(
            src_ref=source,
            dst_ref=target,
            send_sem=right_send.at[unit, hop],
            recv_sem=right_recv.at[unit, hop],
            device_id={"fs": fs + 1},
            device_id_type=MESH,
        )

    def to_left(unit, hop, own=False):
        w = units[unit][0]
        low, piece = unit_rows(unit)
        target = place(w, fs + hop, low, piece)
        source = shards[w].at[pl.ds(low, piece), :] if own else target
        return pltpu.make_async_remote_copy(
            src_ref=source,
            dst_ref=target,
            send_sem=left_send.at[unit, hop],
            recv_sem=left_recv.at[unit, hop],
            device_id={"fs": fs - 1},
            device_id_type=MESH,
        )

    def to_side(unit, side, hop, move):
        w = units[unit][0]
        low, piece = unit_rows(unit)
        block = fs - hop if side == 0 else fs + hop
        target = place(w, block, low, piece)
        return pltpu.make_async_remote_copy(
            src_ref=target,
            dst_ref=target,
            send_sem=side_send.at[unit, side, move - 1, hop],
            recv_sem=side_recv.at[unit, side, move - 1, hop],
            device_id={"grp": lax.rem(grp + move, grp_n)},
            device_id_type=MESH,
        )

    def send_own(unit):
        if unit >= len(units):
            return

        @pl.when(fs < fs_n - 1)
        def _():
            to_right(unit, 0, own=True).start()

        @pl.when(fs > 0)
        def _():
            to_left(unit, 0, own=True).start()

    def relay(unit):
        def step(hop, carry):
            @pl.when(fs >= hop)
            def _():
                to_right(unit, hop - 1).wait_recv()

                @pl.when(fs < fs_n - 1)
                def _():
                    to_right(unit, hop).start()

                for move in range(1, grp_n):
                    to_side(unit, 0, hop, move).start()

            @pl.when(fs + hop < fs_n)
            def _():
                to_left(unit, hop - 1).wait_recv()

                @pl.when(fs > 0)
                def _():
                    to_left(unit, hop).start()

                for move in range(1, grp_n):
                    to_side(unit, 1, hop, move).start()

            return carry

        lax.fori_loop(1, fs_n, step, 0)

    def wait_weight(w):
        own_copy(w).wait()
        for unit in range(len(units)):
            if units[unit][0] == w:

                def step(hop, carry, unit=unit):
                    for move in range(1, grp_n):

                        @pl.when(fs >= hop)
                        def _():
                            to_side(unit, 0, hop, move).wait_recv()

                        @pl.when(fs + hop < fs_n)
                        def _():
                            to_side(unit, 1, hop, move).wait_recv()

                    return carry

                lax.fori_loop(1, fs_n, step, 0)

    def finish_sends():
        for unit in range(len(units)):

            def step(hop, carry, unit=unit):
                @pl.when((fs >= hop) & (fs < fs_n - 1))
                def _():
                    to_right(unit, hop).wait_send()

                @pl.when((fs + hop < fs_n) & (fs > 0))
                def _():
                    to_left(unit, hop).wait_send()

                @pl.when(hop > 0)
                def _():
                    for move in range(1, grp_n):

                        @pl.when(fs >= hop)
                        def _():
                            to_side(unit, 0, hop, move).wait_send()

                        @pl.when(fs + hop < fs_n)
                        def _():
                            to_side(unit, 1, hop, move).wait_send()

                return carry

            lax.fori_loop(0, fs_n, step, 0)

    def other(move, which):
        return lax.rem(chip + move, chips) * 2 + which

    def origin(move, which):
        return lax.rem(chip + chips - move, chips) * 2 + which

    def chunk_rows(owner):
        return pl.ds(aligned(owner * chunk, 16), chunk)

    def column_span(col):
        return pl.ds(aligned(col * column, 128), column)

    def pair_copy(phase, col, move):
        span = column_span(col)
        return pltpu.make_async_remote_copy(
            src_ref=parts.at[phase, chunk_rows(other(move, 1 - core)), span],
            dst_ref=paired.at[phase, move, :, span],
            send_sem=pair_send.at[phase, col, move],
            recv_sem=pair_recv.at[phase, col, move],
            device_id={"tp": twin},
            device_id_type=MESH,
        )

    def sum_copy(phase, col, move):
        span = column_span(col)
        return pltpu.make_async_remote_copy(
            src_ref=outgoing.at[phase, move, :, span],
            dst_ref=landed.at[phase, move, :, span],
            send_sem=sum_send.at[phase, col, move],
            recv_sem=sum_recv.at[phase, col, move],
            device_id={"tp": other(move, core)},
            device_id_type=MESH,
        )

    def piece_span(owner, piece):
        return pl.ds(aligned(owner * chunk + piece * piece_rows, 16), piece_rows)

    def twin_copy(phase, piece):
        rows = piece_span(tp, piece)
        return pltpu.make_async_remote_copy(
            src_ref=streams.at[phase, rows, :],
            dst_ref=streams.at[phase, rows, :],
            send_sem=twin_send.at[phase, piece],
            recv_sem=twin_recv.at[phase, piece],
            device_id={"tp": twin},
            device_id_type=MESH,
        )

    def put_copy(phase, piece, move):
        rows = piece_span(tp, piece)
        return pltpu.make_async_remote_copy(
            src_ref=streams.at[phase, rows, :],
            dst_ref=streams.at[phase, rows, :],
            send_sem=put_send.at[phase, piece, move],
            recv_sem=put_recv.at[phase, piece, move],
            device_id={"tp": other(move, core)},
            device_id_type=MESH,
        )

    def pass_copy(phase, piece, move):
        rows = piece_span(origin(move, core), piece)
        return pltpu.make_async_remote_copy(
            src_ref=streams.at[phase, rows, :],
            dst_ref=streams.at[phase, rows, :],
            send_sem=pass_send.at[phase, piece, move],
            recv_sem=pass_recv.at[phase, piece, move],
            device_id={"tp": twin},
            device_id_type=MESH,
        )

    def gain(row):
        return all_gains[row][...].astype(F32).reshape(1, width)

    def norm_rows(load, row):
        def body(low):
            values = load(pl.ds(low, 32)).astype(F32)
            scale = lax.rsqrt(jnp.mean(values * values, axis=-1, keepdims=True) + 1e-06)
            normed[pl.ds(low, 32), :] = (values * scale * gain(row)).astype(BF16)

        over_rows(count, 32, body)

    def start_sums(phase, col):
        for move in range(1, chips):
            pair_copy(phase, col, move).wait_recv()
            span = column_span(col)
            mine = parts[phase, chunk_rows(other(move, core)), span].astype(F32)
            both = mine + paired[phase, move, :, span].astype(F32)
            outgoing[phase, move, :, span] = both.astype(BF16)
            sum_copy(phase, col, move).start()

    def add_branch(phase, load, row, factor):
        for col in range(columns):
            pair_copy(phase, col, 0).wait_recv()
            for move in range(1, chips):
                sum_copy(phase, col, move).wait_recv()
        for piece in range(piece_n):

            def body(low, piece=piece):
                here = pl.ds(aligned(piece * piece_rows + low, 16), 16)
                rows = pl.ds(aligned(tp * chunk + piece * piece_rows + low, 16), 16)
                total = parts[phase, rows, :].astype(F32) + paired[phase, 0, here, :].astype(F32)
                for move in range(1, chips):
                    total = total + landed[phase, move, here, :].astype(F32)
                scale = lax.rsqrt(jnp.mean(total * total, axis=-1, keepdims=True) + 1e-06)
                branch = total * scale * gain(row)
                streams[phase, rows, :] = (load(rows).astype(F32) + factor * branch).astype(BF16)

            over_rows(piece_rows, 16, body)
            for move in range(1, chips):
                put_copy(phase, piece, move).start()
            twin_copy(phase, piece).start()

    def wait_put(phase):
        for piece in range(piece_n):
            for move in range(1, chips):
                put_copy(phase, piece, move).wait_recv()
                pass_copy(phase, piece, move).start()
        for piece in range(piece_n):
            twin_copy(phase, piece).wait_recv()
            for move in range(1, chips):
                pass_copy(phase, piece, move).wait_recv()

    def finish_phase(phase):
        for col in range(columns):
            for move in range(chips):
                pair_copy(phase, col, move).wait_send()
            for move in range(1, chips):
                sum_copy(phase, col, move).wait_send()
        for piece in range(piece_n):
            twin_copy(phase, piece).wait_send()
            for move in range(1, chips):
                put_copy(phase, piece, move).wait_send()
                pass_copy(phase, piece, move).wait_send()

    def hidden_units():
        def body(low, size):
            cols = pl.ds(low, size)
            gate = jnp.dot(normed[...], gate_full[:, cols], preferred_element_type=F32)
            upper = jnp.dot(normed[...], up_full[:, cols], preferred_element_type=F32)
            hidden[:, cols] = (gate / (1.0 + jnp.exp(-gate)) * upper).astype(BF16)

        over_tiles(hidden.shape[1], body)

    def project(phase, left, right):
        blocks = fs_n // columns

        def step(col, carry):
            terms = [
                jnp.dot(left[...], right[col * blocks + b], preferred_element_type=F32)
                for b in range(blocks)
            ]
            terms = terms[0] if blocks == 1 else jnp.concatenate(terms, axis=1)
            parts[phase, :, column_span(col)] = terms.astype(BF16)
            for move in range(chips - 1, -1, -1):
                pair_copy(phase, col, move).start()

            @pl.when(col > 0)
            def _():
                start_sums(phase, col - 1)

            return carry

        lax.fori_loop(0, columns, step, 0)
        start_sums(phase, columns - 1)

    def mix():
        rows = lax.broadcasted_iota(jnp.int32, (BLOCK, BLOCK), 0)
        cols = lax.broadcasted_iota(jnp.int32, (BLOCK, BLOCK), 1)
        all_spatial_gain = spatial_gain[...].astype(F32).reshape(1, mixed.shape[1])
        for g in range(mixed.shape[1] // GROUP_WIDTH):
            span = slice(g * GROUP_WIDTH, (g + 1) * GROUP_WIDTH)
            v = gelu(jnp.dot(normed[...], v_full[:, span], preferred_element_type=F32))
            u = gelu(jnp.dot(normed[...], u_full[:, span], preferred_element_type=F32))
            v = v - jnp.mean(v, axis=-1, keepdims=True)
            v = v * lax.rsqrt(jnp.mean(v * v, axis=-1, keepdims=True) + 1e-05)
            v = (v * all_spatial_gain[:, span]).astype(BF16)
            weight = spatial_weight[g].astype(F32)
            weight = jnp.where(rows >= cols, weight, 0.0).astype(BF16)
            bias = spatial_bias[...][g : g + 1, :].astype(F32)
            bias = jnp.sum(jnp.where(rows == cols, bias, 0.0), axis=1, keepdims=True)
            for n in range(count // BLOCK):
                part = slice(n * BLOCK, (n + 1) * BLOCK)
                spatial = jnp.dot(weight, v[part], preferred_element_type=F32)
                spatial = spatial + bias
                mixed[part, span] = (u[part] * spatial).astype(BF16)

    load_tokens = lambda rows: tokens[rows, :]
    load_first = lambda rows: streams[0, rows, :]
    load_second = lambda rows: streams[1, rows, :]

    send_own(0)
    send_own(1)
    for w in range(6):
        own_copy(w).start()
    norm_rows(load_tokens, 0)

    for unit in range(5):
        relay(unit)
        send_own(unit + 2)
    wait_weight(0)
    wait_weight(1)
    hidden_units()
    relay(5)
    send_own(7)
    relay(6)
    send_own(8)
    send_own(9)
    wait_weight(2)
    project(0, hidden, down_full)
    relay(7)
    add_branch(0, load_tokens, 1, 0.5)
    relay(8)
    wait_put(0)
    norm_rows(load_first, 2)
    relay(9)
    wait_weight(3)
    wait_weight(4)
    mix()
    wait_weight(5)
    project(1, mixed, out_full)
    add_branch(1, load_first, 3, 1.0)
    wait_put(1)
    norm_rows(load_second, 4)
    hidden_units()
    project(2, hidden, down_full)
    add_branch(2, load_second, 5, 0.5)
    finish_sends()
    wait_put(2)
    last = pltpu.make_async_copy(streams.at[2], result, last_sem)
    last.start()
    for phase in range(3):
        finish_phase(phase)
    last.wait()


def shards(
    sizes,
    tokens,
    ffn_pre_gain,
    gate_weight,
    up_weight,
    down_weight,
    ffn_post_gain,
    mix_pre_gain,
    mix_u_weight,
    mix_v_weight,
    spatial_gain,
    spatial_weight,
    spatial_bias,
    mix_out_weight,
    mix_post_gain,
    late_pre_gain,
    late_post_gain,
):
    grp_n, fs_n, tp_n = sizes
    count, width = tokens.shape
    hidden_width = gate_weight.shape[1]
    channels = mix_u_weight.shape[1]
    columns = math.gcd(fs_n, 4)
    chips = tp_n // 2
    chunk = count // tp_n
    pieces = max(1, chunk // PIECE)
    vmem = pl.BlockSpec(memory_space=pltpu.VMEM)
    hbm = pl.BlockSpec(memory_space=pl.ANY)
    units = sum(SPLITS)
    dma = pltpu.SemaphoreType.DMA
    return pl.pallas_call(
        functools.partial(kernel, sizes),
        out_shape=jax.ShapeDtypeStruct((count, width), BF16),
        in_specs=[vmem] * 7 + [hbm, hbm, hbm, hbm, hbm, hbm, vmem, vmem, vmem],
        out_specs=hbm,
        scratch_shapes=[
            pltpu.VMEM((width, hidden_width), BF16),
            pltpu.VMEM((width, hidden_width), BF16),
            pltpu.VMEM((fs_n,) + down_weight.shape, BF16),
            pltpu.VMEM((width, channels), BF16),
            pltpu.VMEM((width, channels), BF16),
            pltpu.VMEM((fs_n,) + mix_out_weight.shape, BF16),
            pltpu.VMEM((count, width), BF16),
            pltpu.VMEM((count, hidden_width), BF16),
            pltpu.VMEM((count, channels), BF16),
            pltpu.VMEM((3, count, width), BF16),
            pltpu.VMEM((3, chips, chunk, width), BF16),
            pltpu.VMEM((3, chips, chunk, width), BF16),
            pltpu.VMEM((3, chips, chunk, width), BF16),
            pltpu.VMEM((3, count, width), BF16),
            dma((6,)),
            dma((units, fs_n)),
            dma((units, fs_n)),
            dma((units, fs_n)),
            dma((units, fs_n)),
            dma((units, 2, grp_n - 1, fs_n)),
            dma((units, 2, grp_n - 1, fs_n)),
            dma((3, columns, chips)),
            dma((3, columns, chips)),
            dma((3, columns, chips)),
            dma((3, columns, chips)),
            dma((3, pieces)),
            dma((3, pieces)),
            dma((3, pieces, chips)),
            dma((3, pieces, chips)),
            dma((3, pieces, chips)),
            dma((3, pieces, chips)),
            dma(()),
        ],
        compiler_params=pltpu.CompilerParams(
            collective_id=0, has_side_effects=True, vmem_limit_bytes=60 * 2**20
        ),
    )(
        tokens,
        ffn_pre_gain,
        ffn_post_gain,
        mix_pre_gain,
        mix_post_gain,
        late_pre_gain,
        late_post_gain,
        gate_weight,
        up_weight,
        down_weight,
        mix_u_weight,
        mix_v_weight,
        mix_out_weight,
        spatial_gain,
        spatial_weight,
        spatial_bias,
    )


def solution(mesh):
    in_specs = (
        P(("grp", "fs"), None),
        P(),
        P("fs", "tp"),
        P("fs", "tp"),
        P("tp", "fs"),
        P(),
        P(),
        P("fs", "tp"),
        P("fs", "tp"),
        P("tp"),
        P("tp", None, None),
        P("tp", None),
        P("tp", "fs"),
        P(),
        P(),
        P(),
    )
    out_specs = P(("grp", "fs"), None)
    sizes = (mesh.shape["grp"], mesh.shape["fs"], mesh.shape["tp"])
    body = functools.partial(shards, sizes)
    return jax.shard_map(body, mesh=mesh, in_specs=in_specs, out_specs=out_specs, check_vma=False)
```

profile of v0, /device:TPU:1, one launch (start us, length us, event | category | flops | bytes accessed | tf_op | source)
XLA Modules:
  0.0 262.6 jit_solution(7998717207873491789)
XLA Ops:
  0.0 260.3 %shard_map.154 = bf16[256,2048]{1,0:T(8,128)(2,1)} custom-call(bf16[256,2048]{1,0:T(8,128)(2,1)} %tokens.1, bf16[2048]{0:T(1024)(128)(2,1)} %gain0.1, bf16[2048]{0:T(1024)(128)(2,1)} %gain1.1, bf16[2048]{0:T(1024)(128)(2,1)} %gain2.1, bf16[2048]{0:T(1024)(128)(2,1)} %gain3.1, bf16[2048]{0:T(1024)(128)(2,1)} %gain4.1, bf16[2048]{0:T(1024)(128)(2,1)} %gain5.1, ...), custom_call_target="tpu_custom_call" | custom-call | tf_op jit(solution)/shard_map/pallas_call | solution.py:548
  260.3 2.3 copy.18
where the time goes:
time: 263 us
  Pallas kernels  260 us (99%)
    pallas_call x1, Pallas kernels, shards(): pl.pallas_call(functools.partial(kernel, sizes), out_shape=jax.ShapeDtype...  260 us

commit v1 on v0

--- a/solution.py
+++ b/solution.py
@@ -607,6 +607,759 @@
     )
 
 
+FFN_PAIR = "far"
+MIX_PAIR = "near"
+PIECES = (2, 2, 2, 1, 1, 1)
+AHEAD = 2
+ROW_SPLIT = (2, 5)
+
+
+def halves(size):
+    small = size // 256 * 128
+    return small, size - 2 * small
+
+
+def weight_units(shapes, grp_n):
+    units = []
+    for group in ((0, 1), (2,), (3,), (4,), (5,)):
+        made = []
+        for w in group:
+            rows, cols = shapes[w]
+            split = w in ROW_SPLIT
+            small, extra = halves(rows if split else cols)
+            span = small if split else rows
+            share = span // grp_n
+            piece = share // PIECES[w]
+            mine = []
+            for n in range(PIECES[w]):
+                width = cols if split else small
+                mine.append((w, n * piece, share, piece, 0, width, False))
+            if extra and split:
+                mine.append((w, small, extra // grp_n, extra // grp_n, 0, cols, True))
+            elif extra:
+                mine.append((w, 0, rows // grp_n, rows // grp_n, small, extra, True))
+            made.append(mine)
+        for n in range(max(len(mine) for mine in made)):
+            units += [mine[n] for mine in made if n < len(mine)]
+    return units
+
+
+def shared_kernel(
+    sizes,
+    units,
+    tokens,
+    gain0,
+    gain1,
+    gain2,
+    gain3,
+    gain4,
+    gain5,
+    gate_w,
+    up_w,
+    down_w,
+    u_w,
+    v_w,
+    out_w,
+    spatial_gain,
+    spatial_weight,
+    spatial_bias,
+    result,
+    gate_full,
+    up_full,
+    down_full,
+    u_full,
+    v_full,
+    out_full,
+    normed,
+    hidden,
+    mixed,
+    streams,
+    parts,
+    paired,
+    outgoing,
+    landed,
+    crossing,
+    crossed,
+    own_sem,
+    fresh_send,
+    relay_send,
+    relay_recv,
+    side_send,
+    side_recv,
+    pair_send,
+    pair_recv,
+    sum_send,
+    sum_recv,
+    cross_send,
+    cross_recv,
+    put_send,
+    put_recv,
+    last_sem,
+):
+    grp_n, fs_n, tp_n = sizes
+    grp, fs, tp = lax.axis_index("grp"), lax.axis_index("fs"), lax.axis_index("tp")
+    shards = (gate_w, up_w, down_w, u_w, v_w, out_w)
+    fulls = (gate_full, up_full, down_full, u_full, v_full, out_full)
+    count, width = tokens.shape
+    chunk = count // tp_n
+    chips = tp_n // 2
+    chip, core = tp // 2, lax.rem(tp, 2)
+    twin = tp + 1 - 2 * core
+    across = (1 - chip) * 2 + core
+    spot = core * chips + chip
+    far_spot = core * chips + 1 - chip
+    columns = pair_send.shape[2]
+    column = width // columns
+    piece_n = put_send.shape[2]
+    piece_rows = chunk // piece_n
+    all_gains = (gain0, gain1, gain2, gain3, gain4, gain5)
+    middle = fs_n // 2
+
+    class Near:
+        half = lax.rem(fs, 2)
+        partner = fs + 1 - 2 * lax.rem(fs, 2)
+        reach = 2
+        left_ok, right_ok = fs >= 2, fs + 2 < fs_n
+        other_left, other_right = (fs >= 1, fs - 1), (fs + 1 < fs_n, fs + 1)
+
+    class Far:
+        half = fs // middle
+        partner = lax.rem(fs + middle, fs_n)
+        reach = 1
+        left_ok, right_ok = lax.rem(fs, middle) > 0, lax.rem(fs, middle) < middle - 1
+        other_left, other_right = (fs >= middle, middle - 1), (fs < middle, middle)
+
+    named = {"near": Near, "far": Far}
+    ffn, mixer = named[FFN_PAIR], named[MIX_PAIR]
+    pairs = (ffn, ffn, ffn, mixer, mixer, mixer)
+    phases = (ffn, mixer, ffn)
+
+    barrier = pltpu.get_barrier_semaphore()
+    for move in range(1, fs_n):
+        pl.semaphore_signal(
+            barrier, inc=1, device_id={"fs": lax.rem(fs + move, fs_n)}, device_id_type=MESH
+        )
+    for move in range(1, grp_n):
+        pl.semaphore_signal(
+            barrier, inc=1, device_id={"grp": lax.rem(grp + move, grp_n)}, device_id_type=MESH
+        )
+    for move in range(1, tp_n):
+        pl.semaphore_signal(
+            barrier, inc=1, device_id={"tp": lax.rem(tp + move, tp_n)}, device_id_type=MESH
+        )
+    pl.semaphore_wait(barrier, fs_n - 1 + grp_n - 1 + tp_n - 1)
+
+    def large(half):
+        return (half + core) % 2 == 0
+
+    def half_start(w, half):
+        small, extra = halves(shards[w].shape[0 if w in ROW_SPLIT else 1])
+        return half * (small + extra * (1 - core))
+
+    def view(unit, block):
+        w, low, share, rows, col, cols, _ = units[unit]
+        start = low + grp * share
+        if w in ROW_SPLIT:
+            return fulls[w].at[block, pl.ds(aligned(start, 16), rows), :]
+        start = aligned(block * shards[w].shape[0] + start, 16)
+        return fulls[w].at[pl.ds(start, rows), pl.ds(col, cols)]
+
+    def shard_view(unit, half):
+        w, low, share, rows, col, cols, _ = units[unit]
+        start = low + grp * share
+        base = half_start(w, half)
+        if w in ROW_SPLIT:
+            return shards[w].at[pl.ds(aligned(base + start, 16), rows), :]
+        return shards[w].at[pl.ds(aligned(start, 16), rows), pl.ds(aligned(base + col, 128), cols)]
+
+    def has(unit, half):
+        return large(half) if units[unit][6] else True
+
+    def own_copies(w):
+        half = pairs[w].half
+        base = half_start(w, half)
+        small, extra = halves(shards[w].shape[0 if w in ROW_SPLIT else 1])
+
+        def part(low, size, sem):
+            if w in ROW_SPLIT:
+                source = shards[w].at[pl.ds(aligned(base + low, 128), size), :]
+                target = fulls[w].at[fs, pl.ds(low, size), :]
+            else:
+                rows = shards[w].shape[0]
+                source = shards[w].at[:, pl.ds(aligned(base + low, 128), size)]
+                target = fulls[w].at[pl.ds(aligned(fs * rows, 16), rows), pl.ds(low, size)]
+            return pltpu.make_async_copy(source, target, own_sem.at[w, sem])
+
+        made = [(True, part(0, small, 0))]
+        if extra:
+            made.append((large(half), part(small, extra, 1)))
+        return made
+
+    def guarded(ok, act):
+        if ok is True:
+            act()
+        else:
+            pl.when(ok)(act)
+
+    def both(a, b):
+        if a is True:
+            return b
+        if b is True:
+            return a
+        return a & b
+
+    def fresh_copies(unit):
+        pair = pairs[units[unit][0]]
+        block = view(unit, fs)
+
+        def made(slot, half, target):
+            return pltpu.make_async_remote_copy(
+                src_ref=shard_view(unit, half),
+                dst_ref=block,
+                send_sem=fresh_send.at[unit, slot],
+                recv_sem=relay_recv.at[unit, fs],
+                device_id={"fs": target},
+                device_id_type=MESH,
+            )
+
+        own, other = pair.half, 1 - pair.half
+        near, away = has(unit, own), has(unit, other)
+        return (
+            (both(pair.left_ok, near), lambda: made(0, own, fs - pair.reach)),
+            (both(pair.right_ok, near), lambda: made(1, own, fs + pair.reach)),
+            (both(pair.other_left[0], away), lambda: made(2, other, pair.other_left[1])),
+            (both(pair.other_right[0], away), lambda: made(3, other, pair.other_right[1])),
+        )
+
+    def send_own(unit):
+        if unit < len(units):
+            for ok, copy in fresh_copies(unit):
+                guarded(ok, lambda copy=copy: copy().start())
+
+    def relay_copy(unit, block, leftward):
+        pair = pairs[units[unit][0]]
+        target = view(unit, block)
+        return pltpu.make_async_remote_copy(
+            src_ref=target,
+            dst_ref=target,
+            send_sem=relay_send.at[unit, block],
+            recv_sem=relay_recv.at[unit, block],
+            device_id={"fs": fs - pair.reach if leftward else fs + pair.reach},
+            device_id_type=MESH,
+        )
+
+    def side_copy(unit, block, move):
+        target = view(unit, block)
+        return pltpu.make_async_remote_copy(
+            src_ref=target,
+            dst_ref=target,
+            send_sem=side_send.at[unit, move - 1, block],
+            recv_sem=side_recv.at[unit, move - 1, block],
+            device_id={"grp": lax.rem(grp + move, grp_n)},
+            device_id_type=MESH,
+        )
+
+    def over_blocks(unit, act):
+        def whole():
+            def step(d, carry):
+                @pl.when(fs + d < fs_n)
+                def _():
+                    act(fs + d, True)
+
+                @pl.when(fs >= d)
+                def _():
+                    act(fs - d, False)
+
+                return carry
+
+            lax.fori_loop(1, fs_n, step, 0)
+
+        pair = pairs[units[unit][0]]
+        guarded(has(unit, pair.half), whole)
+
+    def relay(unit):
+        pair = pairs[units[unit][0]]
+
+        def act(block, leftward):
+            relay_copy(unit, block, leftward).wait_recv()
+
+            @pl.when(pair.left_ok if leftward else pair.right_ok)
+            def _():
+                relay_copy(unit, block, leftward).start()
+
+            for move in range(1, grp_n):
+                side_copy(unit, block, move).start()
+
+        over_blocks(unit, act)
+        send_own(unit + AHEAD)
+
+    def wait_weight(w):
+        for ok, copy in own_copies(w):
+            guarded(ok, copy.wait)
+        for unit in range(len(units)):
+            if units[unit][0] == w:
+
+                def act(block, leftward, unit=unit):
+                    for move in range(1, grp_n):
+                        side_copy(unit, block, move).wait_recv()
+
+                over_blocks(unit, act)
+
+    def finish_sends():
+        for unit in range(len(units)):
+            pair = pairs[units[unit][0]]
+            for ok, copy in fresh_copies(unit):
+                guarded(ok, lambda copy=copy: copy().wait_send())
+
+            def act(block, leftward, unit=unit, pair=pair):
+                @pl.when(pair.left_ok if leftward else pair.right_ok)
+                def _():
+                    relay_copy(unit, block, leftward).wait_send()
+
+                for move in range(1, grp_n):
+                    side_copy(unit, block, move).wait_send()
+
+            over_blocks(unit, act)
+
+    def column_span(col):
+        return pl.ds(aligned(col * column, 128), column)
+
+    def side_of(phase, turn):
+        half = phases[phase].half
+        return half + (1 - 2 * half) * (1 - turn)
+
+    def pair_copy(phase, turn, col):
+        span = column_span(col)
+        low = side_of(phase, turn) * count + (1 - core) * (count // 2)
+        return pltpu.make_async_remote_copy(
+            src_ref=parts.at[phase, pl.ds(aligned(low, 16), count // 2), span],
+            dst_ref=paired.at[phase, turn, :, span],
+            send_sem=pair_send.at[phase, turn, col],
+            recv_sem=pair_recv.at[phase, turn, col],
+            device_id={"tp": twin},
+            device_id_type=MESH,
+        )
+
+    def sum_copy(phase, turn, col):
+        span = column_span(col)
+        return pltpu.make_async_remote_copy(
+            src_ref=outgoing.at[phase, turn, :, span],
+            dst_ref=landed.at[phase, turn, :, span],
+            send_sem=sum_send.at[phase, turn, col],
+            recv_sem=sum_recv.at[phase, turn, col],
+            device_id={"tp": across},
+            device_id_type=MESH,
+        )
+
+    def cross_copy(phase, col):
+        span = column_span(col)
+        return pltpu.make_async_remote_copy(
+            src_ref=crossing.at[phase, :, span],
+            dst_ref=crossed.at[phase, :, span],
+            send_sem=cross_send.at[phase, col],
+            recv_sem=cross_recv.at[phase, col],
+            device_id={"fs": phases[phase].partner},
+            device_id_type=MESH,
+        )
+
+    def put_copy(phase, which, piece):
+        half = phases[phase].half if phase < 3 else 0
+        side = 1 - half if which in (3, 4, 6) else half
+        place = far_spot if which in (5, 6) else spot
+        start = side * count + place * chunk + piece * piece_rows
+        rows = normed.at[phase, pl.ds(aligned(start, 16), piece_rows), :]
+        if which in (0, 3):
+            target = {"tp": across}
+        elif which == 1:
+            target = {"fs": phases[phase].partner}
+        else:
+            target = {"tp": twin}
+        return pltpu.make_async_remote_copy(
+            src_ref=rows,
+            dst_ref=rows,
+            send_sem=put_send.at[phase, which, piece],
+            recv_sem=put_recv.at[phase, which, piece],
+            device_id=target,
+            device_id_type=MESH,
+        )
+
+    own_puts = ((1,), (0, 1, 2), (0, 1, 2), (0, 2))
+    all_puts = ((1, 3, 4, 6), (0, 1, 2, 3, 4, 5, 6), (0, 1, 2, 3, 4, 5, 6), (0, 2, 5))
+
+    def start_puts(phase, piece):
+        for which in (1, 0, 2):
+            if which in own_puts[phase]:
+                put_copy(phase, which, piece).start()
+
+    def pass_puts(phase):
+        for piece in range(piece_n):
+            if 1 in all_puts[phase]:
+                put_copy(phase, 1, piece).wait_recv()
+                put_copy(phase, 3, piece).start()
+                put_copy(phase, 4, piece).start()
+            if 0 in all_puts[phase]:
+                put_copy(phase, 0, piece).wait_recv()
+                put_copy(phase, 5, piece).start()
+        for piece in range(piece_n):
+            if 3 in all_puts[phase]:
+                put_copy(phase, 3, piece).wait_recv()
+                put_copy(phase, 6, piece).start()
+
+    def wait_puts(phase):
+        for which in (2, 4, 5, 6):
+            if which in all_puts[phase]:
+                for piece in range(piece_n):
+                    put_copy(phase, which, piece).wait_recv()
+
+    def finish_phase(phase):
+        def step(col, carry):
+            for turn in range(2):
+                pair_copy(phase, turn, col).wait_send()
+                sum_copy(phase, turn, col).wait_send()
+            cross_copy(phase, col).wait_send()
+            return carry
+
+        lax.fori_loop(0, columns, step, 0)
+
+    def finish_puts(phase):
+        for which in all_puts[phase]:
+            for piece in range(piece_n):
+                put_copy(phase, which, piece).wait_send()
+
+    def gain(row):
+        return all_gains[row][...].astype(F32).reshape(1, width)
+
+    def scaled(values, row):
+        scale = lax.rsqrt(jnp.mean(values * values, axis=-1, keepdims=True) + 1e-06)
+        return values * scale * gain(row)
+
+    def norm_tokens(start, size):
+        base = ffn.half * count
+
+        def body(low):
+            here = aligned(start + low, 16)
+            values = tokens[pl.ds(here, 16), :].astype(F32)
+            target = pl.ds(aligned(base + start + low, 16), 16)
+            normed[0, target, :] = scaled(values, 0).astype(BF16)
+
+        over_rows(size, 16, body)
+
+    def pass_sum(phase, turn, col):
+        span = column_span(col)
+        pair_copy(phase, turn, col).wait_recv()
+        low = side_of(phase, turn) * count + far_spot * chunk
+        mine = parts[phase, pl.ds(aligned(low, 16), chunk), span].astype(F32)
+        here = pl.ds(aligned((1 - chip) * chunk, 16), chunk)
+        total = mine + paired[phase, turn, here, span].astype(F32)
+        outgoing[phase, turn, :, span] = total.astype(BF16)
+        sum_copy(phase, turn, col).start()
+
+    def cross_sums(phase):
+        def step(col, carry):
+            span = column_span(col)
+            sum_copy(phase, 0, col).wait_recv()
+            low = side_of(phase, 0) * count + spot * chunk
+            mine = parts[phase, pl.ds(aligned(low, 16), chunk), span].astype(F32)
+            here = pl.ds(aligned(chip * chunk, 16), chunk)
+            total = mine + paired[phase, 0, here, span].astype(F32)
+            total = total + landed[phase, 0, :, span].astype(F32)
+            crossing[phase, :, span] = total.astype(BF16)
+            cross_copy(phase, col).start()
+            return carry
+
+        lax.fori_loop(0, columns, step, 0)
+
+    def add_branch(phase, load, row, factor):
+        def wait(col, carry):
+            sum_copy(phase, 1, col).wait_recv()
+            cross_copy(phase, col).wait_recv()
+            return carry
+
+        lax.fori_loop(0, columns, wait, 0)
+        half = phases[phase].half
+        after = phases[phase + 1].half if phase < 2 else 0
+        for piece in range(piece_n):
+
+            def body(low, piece=piece):
+                inside = aligned(piece * piece_rows + low, 16)
+                rows = pl.ds(inside, 16)
+                low = half * count + spot * chunk + inside
+                total = parts[phase, pl.ds(aligned(low, 16), 16), :].astype(F32)
+                here = pl.ds(aligned(chip * chunk + inside, 16), 16)
+                total = total + paired[phase, 1, here, :].astype(F32)
+                total = total + landed[phase, 1, rows, :].astype(F32)
+                total = total + crossed[phase, rows, :].astype(F32)
+                value = load(inside).astype(F32) + factor * scaled(total, row)
+                value = value.astype(BF16)
+                target = pl.ds(aligned(after * count + spot * chunk + inside, 16), 16)
+                if phase < 2:
+                    streams[phase, rows, :] = value
+                    value = scaled(value.astype(F32), row + 1).astype(BF16)
+                normed[phase + 1, target, :] = value
+
+            over_rows(piece_rows, 16, body)
+            start_puts(phase + 1, piece)
+
+    def hidden_tile(phase, rows, cols):
+        left = normed[phase, rows, :]
+        gate = jnp.dot(left, gate_full[:, cols], preferred_element_type=F32)
+        upper = jnp.dot(left, up_full[:, cols], preferred_element_type=F32)
+        hidden[rows, cols] = (gate / (1.0 + jnp.exp(-gate)) * upper).astype(BF16)
+
+    def hidden_half(phase, side):
+        rows = pl.ds(aligned(side * count, 16), count)
+        over_tiles(hidden.shape[1], lambda low, size: hidden_tile(phase, rows, pl.ds(low, size)))
+
+    def project(phase, left, right):
+        def step(i, carry):
+            turn, col = i // columns, lax.rem(i, columns)
+            rows = pl.ds(aligned(side_of(phase, turn) * count, 16), count)
+            per = fs_n // columns
+            terms = [
+                jnp.dot(left[rows, :], right[col * per + b], preferred_element_type=F32)
+                for b in range(per)
+            ]
+            terms = terms[0] if per == 1 else jnp.concatenate(terms, axis=1)
+            parts[phase, rows, column_span(col)] = terms.astype(BF16)
+            pair_copy(phase, turn, col).start()
+
+            @pl.when(i > 0)
+            def _():
+                pass_sum(phase, (i - 1) // columns, lax.rem(i - 1, columns))
+
+            return carry
+
+        lax.fori_loop(0, 2 * columns, step, 0)
+        pass_sum(phase, 1, columns - 1)
+
+    def mix(side):
+        at = lax.broadcasted_iota(jnp.int32, (BLOCK, BLOCK), 0)
+        to = lax.broadcasted_iota(jnp.int32, (BLOCK, BLOCK), 1)
+        half = mixer.half
+        here = mixed.shape[1]
+        groups = here // GROUP_WIDTH
+        all_gain = spatial_gain[...].astype(F32).reshape(1, 2 * here)
+        all_gain = jnp.where(half == 0, all_gain[:, :here], all_gain[:, here:])
+        all_bias = spatial_bias[...].astype(F32)
+        all_bias = jnp.where(half == 0, all_bias[:groups], all_bias[groups:])
+
+        def block(n, carry):
+            rows = pl.ds(aligned(side * count + n * BLOCK, 16), BLOCK)
+            left = normed[1, rows, :]
+            every_v = gelu(jnp.dot(left, v_full[...], preferred_element_type=F32))
+            every_u = gelu(jnp.dot(left, u_full[...], preferred_element_type=F32))
+            for g in range(groups):
+                span = slice(g * GROUP_WIDTH, (g + 1) * GROUP_WIDTH)
+                v = every_v[:, span]
+                v = v - jnp.mean(v, axis=-1, keepdims=True)
+                v = v * lax.rsqrt(jnp.mean(v * v, axis=-1, keepdims=True) + 1e-05)
+                v = (v * all_gain[:, span]).astype(BF16)
+                weight = spatial_weight[half * groups + g].astype(F32)
+                weight = jnp.where(at >= to, weight, 0.0).astype(BF16)
+                bias = jnp.where(at == to, all_bias[g : g + 1, :], 0.0)
+                bias = jnp.sum(bias, axis=1, keepdims=True)
+                spatial = jnp.dot(weight, v, preferred_element_type=F32) + bias
+                mixed[rows, span] = (every_u[:, span] * spatial).astype(BF16)
+            return carry
+
+        lax.fori_loop(0, count // BLOCK, block, 0)
+
+    def load_tokens(low):
+        return tokens[pl.ds(aligned(spot * chunk + low, 16), 16), :]
+
+    def load_stream(phase):
+        return lambda low: streams[phase, pl.ds(low, 16), :]
+
+    last = [unit for unit in range(len(units)) if units[unit][0] < 2][-1]
+    downs = [unit for unit in range(len(units)) if units[unit][0] == 2]
+    first = [unit for unit in range(len(units)) if units[unit][0] == 3]
+    second = [unit for unit in range(len(units)) if units[unit][0] == 4]
+    third = [unit for unit in range(len(units)) if units[unit][0] == 5]
+
+    def relays(some):
+        for unit in some:
+            relay(unit)
+
+    for unit in range(AHEAD):
+        send_own(unit)
+    for w in range(6):
+        for ok, copy in own_copies(w):
+            guarded(ok, copy.start)
+    norm_tokens(spot * chunk, chunk)
+    for piece in range(piece_n):
+        start_puts(0, piece)
+
+    small, extra = halves(gate_w.shape[1])
+    if extra:
+
+        @pl.when(jnp.logical_not(large(ffn.half)))
+        def _():
+            for full in (gate_full, up_full):
+                full[:, pl.ds(small, extra)] = jnp.zeros((full.shape[0], extra), BF16)
+            pad = jnp.zeros((fs_n, extra, down_full.shape[2]), BF16)
+            down_full[:, pl.ds(small, extra), :] = pad
+
+    for move in range(1, tp_n):
+        norm_tokens(lax.rem(spot + move, tp_n) * chunk, chunk)
+
+    relay(0)
+    pass_puts(0)
+    relays(range(1, last + 1))
+    wait_puts(0)
+    wait_weight(0)
+    wait_weight(1)
+    relay(downs[0])
+    hidden_half(0, ffn.half)
+    relays(downs[1:2])
+    hidden_half(0, 1 - ffn.half)
+    relays(downs[2:])
+    wait_weight(2)
+    project(0, hidden, down_full)
+    relays(first)
+    cross_sums(0)
+    relays(second)
+    add_branch(0, load_tokens, 1, 0.5)
+    relays(third)
+    pass_puts(1)
+    wait_weight(3)
+    wait_weight(4)
+    wait_puts(1)
+    mix(mixer.half)
+    mix(1 - mixer.half)
+    wait_weight(5)
+    project(1, mixed, out_full)
+    cross_sums(1)
+    add_branch(1, load_stream(0), 3, 1.0)
+    pass_puts(2)
+    wait_puts(2)
+    hidden_half(2, ffn.half)
+    hidden_half(2, 1 - ffn.half)
+    project(2, hidden, down_full)
+    cross_sums(2)
+    add_branch(2, load_stream(1), 5, 0.5)
+    pass_puts(3)
+    finish_sends()
+    for phase in range(3):
+        finish_phase(phase)
+        finish_puts(phase)
+    wait_puts(3)
+    copy = pltpu.make_async_copy(normed.at[3, pl.ds(0, count), :], result, last_sem)
+    copy.start()
+    finish_puts(3)
+    copy.wait()
+
+
+def shared(
+    sizes,
+    tokens,
+    ffn_pre_gain,
+    gate_weight,
+    up_weight,
+    down_weight,
+    ffn_post_gain,
+    mix_pre_gain,
+    mix_u_weight,
+    mix_v_weight,
+    spatial_gain,
+    spatial_weight,
+    spatial_bias,
+    mix_out_weight,
+    mix_post_gain,
+    late_pre_gain,
+    late_post_gain,
+):
+    grp_n, fs_n, tp_n = sizes
+    count, width = tokens.shape
+    small, extra = halves(gate_weight.shape[1])
+    hidden_width = small + extra
+    channels = mix_u_weight.shape[1] // 2
+    columns = math.gcd(fs_n, 4)
+    chunk = count // tp_n
+    pieces = max(1, chunk // PIECE)
+    vmem = pl.BlockSpec(memory_space=pltpu.VMEM)
+    hbm = pl.BlockSpec(memory_space=pl.ANY)
+    weights = (gate_weight, up_weight, down_weight, mix_u_weight, mix_v_weight, mix_out_weight)
+    units = weight_units([w.shape for w in weights], grp_n)
+    unit_n = len(units)
+    dma = pltpu.SemaphoreType.DMA
+    return pl.pallas_call(
+        functools.partial(shared_kernel, sizes, units),
+        out_shape=jax.ShapeDtypeStruct((count, width), BF16),
+        in_specs=[vmem] * 7 + [hbm, hbm, hbm, hbm, hbm, hbm, vmem, vmem, vmem],
+        out_specs=hbm,
+        scratch_shapes=[
+            pltpu.VMEM((width, hidden_width), BF16),
+            pltpu.VMEM((width, hidden_width), BF16),
+            pltpu.VMEM((fs_n, hidden_width, down_weight.shape[1]), BF16),
+            pltpu.VMEM((width, channels), BF16),
+            pltpu.VMEM((width, channels), BF16),
+            pltpu.VMEM((fs_n, channels, mix_out_weight.shape[1]), BF16),
+            pltpu.VMEM((4, 2 * count, width), BF16),
+            pltpu.VMEM((2 * count, hidden_width), BF16),
+            pltpu.VMEM((2 * count, channels), BF16),
+            pltpu.VMEM((2, chunk, width), BF16),
+            pltpu.VMEM((3, 2 * count, width), BF16),
+            pltpu.VMEM((3, 2, count // 2, width), BF16),
+            pltpu.VMEM((3, 2, chunk, width), BF16),
+            pltpu.VMEM((3, 2, chunk, width), BF16),
+            pltpu.VMEM((3, chunk, width), BF16),
+            pltpu.VMEM((3, chunk, width), BF16),
+            dma((6, 2)),
+            dma((unit_n, 4)),
+            dma((unit_n, fs_n)),
+            dma((unit_n, fs_n)),
+            dma((unit_n, max(1, grp_n - 1), fs_n)),
+            dma((unit_n, max(1, grp_n - 1), fs_n)),
+            dma((3, 2, columns)),
+            dma((3, 2, columns)),
+            dma((3, 2, columns)),
+            dma((3, 2, columns)),
+            dma((3, columns)),
+            dma((3, columns)),
+            dma((4, 7, pieces)),
+            dma((4, 7, pieces)),
+            dma(()),
+        ],
+        compiler_params=pltpu.CompilerParams(
+            collective_id=0, has_side_effects=True, vmem_limit_bytes=60 * 2**20
+        ),
+    )(
+        tokens,
+        ffn_pre_gain,
+        ffn_post_gain,
+        mix_pre_gain,
+        mix_post_gain,
+        late_pre_gain,
+        late_post_gain,
+        gate_weight,
+        up_weight,
+        down_weight,
+        mix_u_weight,
+        mix_v_weight,
+        mix_out_weight,
+        spatial_gain,
+        spatial_weight,
+        spatial_bias,
+    )
+
+
+def can_share(sizes, tokens, gate_weight, mix_u_weight):
+    grp_n, fs_n, tp_n = sizes
+    count = tokens.shape[0] // (grp_n * fs_n)
+    rows = gate_weight.shape[0] // fs_n
+    hidden_width = gate_weight.shape[1] // tp_n
+    channels = mix_u_weight.shape[1] // tp_n
+    return (
+        tp_n == 4
+        and fs_n == 4
+        and count % (4 * PIECE) == 0
+        and rows % (32 * grp_n) == 0
+        and hidden_width % 128 == 0
+        and halves(hidden_width)[0] % (32 * grp_n) == 0
+        and channels % (2 * GROUP_WIDTH) == 0
+    )
+
+
 def solution(mesh):
     in_specs = (
         P(("grp", "fs"), None),
@@ -628,5 +1381,12 @@
     )
     out_specs = P(("grp", "fs"), None)
     sizes = (mesh.shape["grp"], mesh.shape["fs"], mesh.shape["tp"])
-    body = functools.partial(shards, sizes)
-    return jax.shard_map(body, mesh=mesh, in_specs=in_specs, out_specs=out_specs, check_vma=False)
+
+    def step(*arrays):
+        plan = shared if can_share(sizes, arrays[0], arrays[2], arrays[7]) else shards
+        body = functools.partial(plan, sizes)
+        return jax.shard_map(
+            body, mesh=mesh, in_specs=in_specs, out_specs=out_specs, check_vma=False
+        )(*arrays)
+
+    return step

time: 263 us -> 214 us (0.81)
  Pallas kernels: 260 us -> 211 us
    pallas_call x1, Pallas kernels: 260 us -> 211 us  [shared(): pl.pallas_call(functools.partial(shared_kernel, sizes, units), out_shape=...]
where the time goes in v1:
time: 214 us
  Pallas kernels  211 us (99%)
  local copies, waits for them, and re-layouts  2.3 us (1%)
    pallas_call x1, Pallas kernels, shared(): pl.pallas_call(functools.partial(shared_kernel, sizes, units), out_shape=...  211 us

profile of v1, /device:TPU:1, one launch (start us, length us, event | category | flops | bytes accessed | tf_op | source)
XLA Modules:
  0.0 213.6 jit_solution(9602099446605918470)
XLA Ops:
  0.0 211.3 %shard_map.154 = bf16[256,2048]{1,0:T(8,128)(2,1)} custom-call(bf16[256,2048]{1,0:T(8,128)(2,1)} %tokens.1, bf16[2048]{0:T(1024)(128)(2,1)} %gain0.1, bf16[2048]{0:T(1024)(128)(2,1)} %gain1.1, bf16[2048]{0:T(1024)(128)(2,1)} %gain2.1, bf16[2048]{0:T(1024)(128)(2,1)} %gain3.1, bf16[2048]{0:T(1024)(128)(2,1)} %gain4.1, bf16[2048]{0:T(1024)(128)(2,1)} %gain5.1, ...), custom_call_target="tpu_custom_call" | custom-call | tf_op jit(solution)/shard_map/pallas_call | solution.py:1285
  211.3 2.3 %copy.18 = bf16[256,2048]{1,0:T(8,128)(2,1)} copy(bf16[256,2048]{1,0:T(8,128)(2,1)} %shard_map.154) | data formatting | bytes 2097152

commit v2 on v1

--- a/solution.py
+++ b/solution.py
@@ -610,7 +610,8 @@
 FFN_PAIR = "far"
 MIX_PAIR = "near"
 PIECES = (2, 2, 2, 1, 1, 1)
-AHEAD = 2
+AHEAD = 3
+LAG = 2
 ROW_SPLIT = (2, 5)
 
 
@@ -701,19 +702,25 @@
     shards = (gate_w, up_w, down_w, u_w, v_w, out_w)
     fulls = (gate_full, up_full, down_full, u_full, v_full, out_full)
     count, width = tokens.shape
-    chunk = count // tp_n
     chips = tp_n // 2
     chip, core = tp // 2, lax.rem(tp, 2)
     twin = tp + 1 - 2 * core
     across = (1 - chip) * 2 + core
     spot = core * chips + chip
     far_spot = core * chips + 1 - chip
-    columns = pair_send.shape[2]
+    columns = pair_recv.shape[2]
     column = width // columns
     piece_n = put_send.shape[2]
-    piece_rows = chunk // piece_n
+    piece_rows = count // piece_n
+    chunk = piece_rows // tp_n
     all_gains = (gain0, gain1, gain2, gain3, gain4, gain5)
     middle = fs_n // 2
+
+    last = [unit for unit in range(len(units)) if units[unit][0] < 2][-1]
+    downs = [unit for unit in range(len(units)) if units[unit][0] == 2]
+    first = [unit for unit in range(len(units)) if units[unit][0] == 3]
+    second = [unit for unit in range(len(units)) if units[unit][0] == 4]
+    third = [unit for unit in range(len(units)) if units[unit][0] == 5]
 
     class Near:
         half = lax.rem(fs, 2)
@@ -824,17 +831,26 @@
 
         own, other = pair.half, 1 - pair.half
         near, away = has(unit, own), has(unit, other)
+        left, right = fs - pair.reach, fs + pair.reach
+        other_left, other_right = pair.other_left[1], pair.other_right[1]
         return (
-            (both(pair.left_ok, near), lambda: made(0, own, fs - pair.reach)),
-            (both(pair.right_ok, near), lambda: made(1, own, fs + pair.reach)),
-            (both(pair.other_left[0], away), lambda: made(2, other, pair.other_left[1])),
-            (both(pair.other_right[0], away), lambda: made(3, other, pair.other_right[1])),
+            (both(pair.left_ok, near), left, lambda: made(0, own, left)),
+            (both(pair.right_ok, near), right, lambda: made(1, own, right)),
+            (both(pair.other_left[0], away), other_left, lambda: made(2, other, other_left)),
+            (both(pair.other_right[0], away), other_right, lambda: made(3, other, other_right)),
         )
 
     def send_own(unit):
-        if unit < len(units):
-            for ok, copy in fresh_copies(unit):
+        if unit < first[0]:
+            for ok, _, copy in fresh_copies(unit):
                 guarded(ok, lambda copy=copy: copy().start())
+
+    def send_some(some, ends):
+        for unit in some:
+            for ok, target, copy in fresh_copies(unit):
+                inner = jnp.logical_and(target > 0, target < fs_n - 1)
+                chosen = jnp.logical_not(inner) if ends else inner
+                guarded(jnp.logical_and(ok, chosen), lambda copy=copy: copy().start())
 
     def relay_copy(unit, block, leftward):
         pair = pairs[units[unit][0]]
@@ -905,10 +921,10 @@
 
                 over_blocks(unit, act)
 
-    def finish_sends():
-        for unit in range(len(units)):
+    def finish_sends(some):
+        for unit in some:
             pair = pairs[units[unit][0]]
-            for ok, copy in fresh_copies(unit):
+            for ok, _, copy in fresh_copies(unit):
                 guarded(ok, lambda copy=copy: copy().wait_send())
 
             def act(block, leftward, unit=unit, pair=pair):
@@ -924,53 +940,67 @@
     def column_span(col):
         return pl.ds(aligned(col * column, 128), column)
 
+    def pair_step(phase, piece, col):
+        span = column_span(col)
+        return pltpu.make_async_remote_copy(
+            src_ref=parts.at[phase, piece, :, 1 - core, :, span],
+            dst_ref=paired.at[phase, piece, :, :, span],
+            send_sem=pair_send.at[phase, piece],
+            recv_sem=pair_recv.at[phase, piece, col],
+            device_id={"tp": twin},
+            device_id_type=MESH,
+        )
+
     def side_of(phase, turn):
         half = phases[phase].half
-        return half + (1 - 2 * half) * (1 - turn)
-
-    def pair_copy(phase, turn, col):
-        span = column_span(col)
-        low = side_of(phase, turn) * count + (1 - core) * (count // 2)
-        return pltpu.make_async_remote_copy(
-            src_ref=parts.at[phase, pl.ds(aligned(low, 16), count // 2), span],
-            dst_ref=paired.at[phase, turn, :, span],
-            send_sem=pair_send.at[phase, turn, col],
-            recv_sem=pair_recv.at[phase, turn, col],
-            device_id={"tp": twin},
-            device_id_type=MESH,
-        )
-
-    def sum_copy(phase, turn, col):
+        return 1 - half if turn == 0 else half
+
+    def sum_step(phase, piece, turn, col):
         span = column_span(col)
         return pltpu.make_async_remote_copy(
-            src_ref=outgoing.at[phase, turn, :, span],
-            dst_ref=landed.at[phase, turn, :, span],
-            send_sem=sum_send.at[phase, turn, col],
-            recv_sem=sum_recv.at[phase, turn, col],
+            src_ref=outgoing.at[phase, piece, turn, :, span],
+            dst_ref=landed.at[phase, piece, turn, :, span],
+            send_sem=sum_send.at[phase, piece],
+            recv_sem=sum_recv.at[phase, piece, turn, col],
             device_id={"tp": across},
             device_id_type=MESH,
         )
 
-    def cross_copy(phase, col):
+    def cross_step(phase, piece, col):
         span = column_span(col)
         return pltpu.make_async_remote_copy(
-            src_ref=crossing.at[phase, :, span],
-            dst_ref=crossed.at[phase, :, span],
-            send_sem=cross_send.at[phase, col],
-            recv_sem=cross_recv.at[phase, col],
+            src_ref=crossing.at[phase, piece, :, span],
+            dst_ref=crossed.at[phase, piece, :, span],
+            send_sem=cross_send.at[phase, piece],
+            recv_sem=cross_recv.at[phase, piece, col],
             device_id={"fs": phases[phase].partner},
             device_id_type=MESH,
         )
+
+    def all_sent(source, target, sem, device):
+        pltpu.make_async_remote_copy(
+            src_ref=source,
+            dst_ref=target,
+            send_sem=sem,
+            recv_sem=pair_recv.at[0, 0, 0],
+            device_id=device,
+            device_id_type=MESH,
+        ).wait_send()
+
+    def group_rows(phase, side, piece, inside, size):
+        start = piece * 2 * piece_rows + side * piece_rows + inside
+        if phase == 3:
+            start = piece * piece_rows + inside
+        return pl.ds(aligned(start, 16), size)
 
     def put_copy(phase, which, piece):
         half = phases[phase].half if phase < 3 else 0
         side = 1 - half if which in (3, 4, 6) else half
-        place = far_spot if which in (5, 6) else spot
-        start = side * count + place * chunk + piece * piece_rows
-        rows = normed.at[phase, pl.ds(aligned(start, 16), piece_rows), :]
+        place = far_spot if which in (5, 6, 7) else spot
+        rows = normed.at[phase, group_rows(phase, side, piece, place * chunk, chunk), :]
         if which in (0, 3):
             target = {"tp": across}
-        elif which == 1:
+        elif which in (1, 7):
             target = {"fs": phases[phase].partner}
         else:
             target = {"tp": twin}
@@ -984,46 +1014,58 @@
         )
 
     own_puts = ((1,), (0, 1, 2), (0, 1, 2), (0, 2))
-    all_puts = ((1, 3, 4, 6), (0, 1, 2, 3, 4, 5, 6), (0, 1, 2, 3, 4, 5, 6), (0, 2, 5))
+    every_put = (0, 1, 2, 3, 4, 5, 6, 7)
+    all_puts = ((1, 3, 4, 6), every_put, every_put, (0, 2, 5))
 
     def start_puts(phase, piece):
         for which in (1, 0, 2):
             if which in own_puts[phase]:
                 put_copy(phase, which, piece).start()
 
-    def pass_puts(phase):
+    def routed(phase, which):
+        split = phase > 0 and phase < 3 and phases[phase] is Near
+        cut = piece_n // 2 if split else piece_n
+        return range(cut) if which == 3 else range(cut, piece_n)
+
+    def pieces_of(phase, which):
+        if which in (3, 7):
+            return routed(phase, which)
+        return range(piece_n)
+
+    def pass_near(phase, piece):
+        put_copy(phase, 1, piece).wait_recv()
+        if piece in routed(phase, 3):
+            put_copy(phase, 3, piece).start()
+        put_copy(phase, 4, piece).start()
+
+    def pass_side(phase, piece):
+        put_copy(phase, 0, piece).wait_recv()
+        if phase < 3 and piece in routed(phase, 7):
+            put_copy(phase, 7, piece).start()
+        put_copy(phase, 5, piece).start()
+
+    def pass_last(phase, piece):
+        put_copy(phase, 3 if piece in routed(phase, 3) else 7, piece).wait_recv()
+        put_copy(phase, 6, piece).start()
+
+    def wait_puts(phase, piece, some):
+        for which in some:
+            put_copy(phase, which, piece).wait_recv()
+
+    def finish_phase(phase):
         for piece in range(piece_n):
-            if 1 in all_puts[phase]:
-                put_copy(phase, 1, piece).wait_recv()
-                put_copy(phase, 3, piece).start()
-                put_copy(phase, 4, piece).start()
-            if 0 in all_puts[phase]:
-                put_copy(phase, 0, piece).wait_recv()
-                put_copy(phase, 5, piece).start()
-        for piece in range(piece_n):
-            if 3 in all_puts[phase]:
-                put_copy(phase, 3, piece).wait_recv()
-                put_copy(phase, 6, piece).start()
-
-    def wait_puts(phase):
-        for which in (2, 4, 5, 6):
-            if which in all_puts[phase]:
-                for piece in range(piece_n):
-                    put_copy(phase, which, piece).wait_recv()
-
-    def finish_phase(phase):
-        def step(col, carry):
-            for turn in range(2):
-                pair_copy(phase, turn, col).wait_send()
-                sum_copy(phase, turn, col).wait_send()
-            cross_copy(phase, col).wait_send()
-            return carry
-
-        lax.fori_loop(0, columns, step, 0)
+            target = paired.at[phase, piece]
+            source = parts.at[phase, piece, :, 1 - core]
+            all_sent(source, target, pair_send.at[phase, piece], {"tp": twin})
+            source, target = outgoing.at[phase, piece], landed.at[phase, piece]
+            all_sent(source, target, sum_send.at[phase, piece], {"tp": across})
+            source, target = crossing.at[phase, piece], crossed.at[phase, piece]
+            device = {"fs": phases[phase].partner}
+            all_sent(source, target, cross_send.at[phase, piece], device)
 
     def finish_puts(phase):
         for which in all_puts[phase]:
-            for piece in range(piece_n):
+            for piece in pieces_of(phase, which):
                 put_copy(phase, which, piece).wait_send()
 
     def gain(row):
@@ -1033,72 +1075,69 @@
         scale = lax.rsqrt(jnp.mean(values * values, axis=-1, keepdims=True) + 1e-06)
         return values * scale * gain(row)
 
-    def norm_tokens(start, size):
-        base = ffn.half * count
-
+    def norm_tokens(piece, start, size):
         def body(low):
-            here = aligned(start + low, 16)
+            here = aligned(piece * piece_rows + start + low, 16)
             values = tokens[pl.ds(here, 16), :].astype(F32)
-            target = pl.ds(aligned(base + start + low, 16), 16)
+            target = group_rows(0, ffn.half, piece, start + low, 16)
             normed[0, target, :] = scaled(values, 0).astype(BF16)
 
         over_rows(size, 16, body)
 
-    def pass_sum(phase, turn, col):
+    def pass_sum(phase, piece, turn, col):
         span = column_span(col)
-        pair_copy(phase, turn, col).wait_recv()
-        low = side_of(phase, turn) * count + far_spot * chunk
-        mine = parts[phase, pl.ds(aligned(low, 16), chunk), span].astype(F32)
+        if turn == 0:
+            pair_step(phase, piece, col).wait_recv()
         here = pl.ds(aligned((1 - chip) * chunk, 16), chunk)
-        total = mine + paired[phase, turn, here, span].astype(F32)
-        outgoing[phase, turn, :, span] = total.astype(BF16)
-        sum_copy(phase, turn, col).start()
-
-    def cross_sums(phase):
+        side = side_of(phase, turn)
+        total = parts[phase, piece, side, core, here, span].astype(F32)
+        total = total + paired[phase, piece, side, here, span].astype(F32)
+        outgoing[phase, piece, turn, :, span] = total.astype(BF16)
+        sum_step(phase, piece, turn, col).start()
+
+    def cross_sums(phase, piece):
+        side = 1 - phases[phase].half
+        here = pl.ds(aligned(chip * chunk, 16), chunk)
+
         def step(col, carry):
             span = column_span(col)
-            sum_copy(phase, 0, col).wait_recv()
-            low = side_of(phase, 0) * count + spot * chunk
-            mine = parts[phase, pl.ds(aligned(low, 16), chunk), span].astype(F32)
-            here = pl.ds(aligned(chip * chunk, 16), chunk)
-            total = mine + paired[phase, 0, here, span].astype(F32)
-            total = total + landed[phase, 0, :, span].astype(F32)
-            crossing[phase, :, span] = total.astype(BF16)
-            cross_copy(phase, col).start()
+            sum_step(phase, piece, 0, col).wait_recv()
+            total = parts[phase, piece, side, core, here, span].astype(F32)
+            total = total + paired[phase, piece, side, here, span].astype(F32)
+            total = total + landed[phase, piece, 0, :, span].astype(F32)
+            crossing[phase, piece, :, span] = total.astype(BF16)
+            cross_step(phase, piece, col).start()
             return carry
 
         lax.fori_loop(0, columns, step, 0)
 
-    def add_branch(phase, load, row, factor):
+    def add_branch(phase, piece, load, row, factor):
         def wait(col, carry):
-            sum_copy(phase, 1, col).wait_recv()
-            cross_copy(phase, col).wait_recv()
+            sum_step(phase, piece, 1, col).wait_recv()
+            cross_step(phase, piece, col).wait_recv()
             return carry
 
         lax.fori_loop(0, columns, wait, 0)
-        half = phases[phase].half
+        side = phases[phase].half
         after = phases[phase + 1].half if phase < 2 else 0
-        for piece in range(piece_n):
-
-            def body(low, piece=piece):
-                inside = aligned(piece * piece_rows + low, 16)
-                rows = pl.ds(inside, 16)
-                low = half * count + spot * chunk + inside
-                total = parts[phase, pl.ds(aligned(low, 16), 16), :].astype(F32)
-                here = pl.ds(aligned(chip * chunk + inside, 16), 16)
-                total = total + paired[phase, 1, here, :].astype(F32)
-                total = total + landed[phase, 1, rows, :].astype(F32)
-                total = total + crossed[phase, rows, :].astype(F32)
-                value = load(inside).astype(F32) + factor * scaled(total, row)
-                value = value.astype(BF16)
-                target = pl.ds(aligned(after * count + spot * chunk + inside, 16), 16)
-                if phase < 2:
-                    streams[phase, rows, :] = value
-                    value = scaled(value.astype(F32), row + 1).astype(BF16)
-                normed[phase + 1, target, :] = value
-
-            over_rows(piece_rows, 16, body)
-            start_puts(phase + 1, piece)
+
+        def body(low):
+            rows = pl.ds(low, 16)
+            here = pl.ds(aligned(chip * chunk + low, 16), 16)
+            total = parts[phase, piece, side, core, here, :].astype(F32)
+            total = total + paired[phase, piece, side, here, :].astype(F32)
+            total = total + landed[phase, piece, 1, rows, :].astype(F32)
+            total = total + crossed[phase, piece, rows, :].astype(F32)
+            value = load(piece, low).astype(F32) + factor * scaled(total, row)
+            value = value.astype(BF16)
+            if phase < 2:
+                streams[phase, pl.ds(aligned(piece * chunk + low, 16), 16), :] = value
+                value = scaled(value.astype(F32), row + 1).astype(BF16)
+            target = group_rows(phase + 1, after, piece, spot * chunk + low, 16)
+            normed[phase + 1, target, :] = value
+
+        over_rows(chunk, 16, body)
+        start_puts(phase + 1, piece)
 
     def hidden_tile(phase, rows, cols):
         left = normed[phase, rows, :]
@@ -1106,33 +1145,45 @@
         upper = jnp.dot(left, up_full[:, cols], preferred_element_type=F32)
         hidden[rows, cols] = (gate / (1.0 + jnp.exp(-gate)) * upper).astype(BF16)
 
-    def hidden_half(phase, side):
-        rows = pl.ds(aligned(side * count, 16), count)
+    def piece_span(piece):
+        return pl.ds(piece * 2 * piece_rows, 2 * piece_rows)
+
+    def hidden_piece(phase, piece):
+        rows = piece_span(piece)
         over_tiles(hidden.shape[1], lambda low, size: hidden_tile(phase, rows, pl.ds(low, size)))
 
-    def project(phase, left, right):
-        def step(i, carry):
-            turn, col = i // columns, lax.rem(i, columns)
-            rows = pl.ds(aligned(side_of(phase, turn) * count, 16), count)
+    def project(phase, piece, left, right):
+        rows = piece_span(piece)
+
+        def step(col, carry):
             per = fs_n // columns
             terms = [
                 jnp.dot(left[rows, :], right[col * per + b], preferred_element_type=F32)
                 for b in range(per)
             ]
             terms = terms[0] if per == 1 else jnp.concatenate(terms, axis=1)
-            parts[phase, rows, column_span(col)] = terms.astype(BF16)
-            pair_copy(phase, turn, col).start()
-
-            @pl.when(i > 0)
+            terms = terms.astype(BF16).reshape(2, 2, chips * chunk, column)
+            parts[phase, piece, :, :, :, column_span(col)] = terms
+            pair_step(phase, piece, col).start()
+
+            @pl.when(col >= LAG)
             def _():
-                pass_sum(phase, (i - 1) // columns, lax.rem(i - 1, columns))
+                pass_sum(phase, piece, 0, col - LAG)
 
             return carry
 
-        lax.fori_loop(0, 2 * columns, step, 0)
-        pass_sum(phase, 1, columns - 1)
-
-    def mix(side):
+        def late(turn):
+            def step(col, carry):
+                pass_sum(phase, piece, turn, col)
+                return carry
+
+            return step
+
+        lax.fori_loop(0, columns, step, 0)
+        lax.fori_loop(columns - LAG, columns, late(0), 0)
+        lax.fori_loop(0, columns, late(1), 0)
+
+    def mix(piece):
         at = lax.broadcasted_iota(jnp.int32, (BLOCK, BLOCK), 0)
         to = lax.broadcasted_iota(jnp.int32, (BLOCK, BLOCK), 1)
         half = mixer.half
@@ -1144,7 +1195,7 @@
         all_bias = jnp.where(half == 0, all_bias[:groups], all_bias[groups:])
 
         def block(n, carry):
-            rows = pl.ds(aligned(side * count + n * BLOCK, 16), BLOCK)
+            rows = pl.ds(aligned(piece * 2 * piece_rows + n * BLOCK, 16), BLOCK)
             left = normed[1, rows, :]
             every_v = gelu(jnp.dot(left, v_full[...], preferred_element_type=F32))
             every_u = gelu(jnp.dot(left, u_full[...], preferred_element_type=F32))
@@ -1162,19 +1213,14 @@
                 mixed[rows, span] = (every_u[:, span] * spatial).astype(BF16)
             return carry
 
-        lax.fori_loop(0, count // BLOCK, block, 0)
-
-    def load_tokens(low):
-        return tokens[pl.ds(aligned(spot * chunk + low, 16), 16), :]
+        lax.fori_loop(0, 2 * piece_rows // BLOCK, block, 0)
+
+    def load_tokens(piece, low):
+        start = piece * piece_rows + spot * chunk + low
+        return tokens[pl.ds(aligned(start, 16), 16), :]
 
     def load_stream(phase):
-        return lambda low: streams[phase, pl.ds(low, 16), :]
-
-    last = [unit for unit in range(len(units)) if units[unit][0] < 2][-1]
-    downs = [unit for unit in range(len(units)) if units[unit][0] == 2]
-    first = [unit for unit in range(len(units)) if units[unit][0] == 3]
-    second = [unit for unit in range(len(units)) if units[unit][0] == 4]
-    third = [unit for unit in range(len(units)) if units[unit][0] == 5]
+        return lambda piece, low: streams[phase, pl.ds(aligned(piece * chunk + low, 16), 16), :]
 
     def relays(some):
         for unit in some:
@@ -1185,8 +1231,8 @@
     for w in range(6):
         for ok, copy in own_copies(w):
             guarded(ok, copy.start)
-    norm_tokens(spot * chunk, chunk)
     for piece in range(piece_n):
+        norm_tokens(piece, spot * chunk, chunk)
         start_puts(0, piece)
 
     small, extra = halves(gate_w.shape[1])
@@ -1199,50 +1245,94 @@
             pad = jnp.zeros((fs_n, extra, down_full.shape[2]), BF16)
             down_full[:, pl.ds(small, extra), :] = pad
 
-    for move in range(1, tp_n):
-        norm_tokens(lax.rem(spot + move, tp_n) * chunk, chunk)
-
-    relay(0)
-    pass_puts(0)
-    relays(range(1, last + 1))
-    wait_puts(0)
+    for piece in range(piece_n):
+        for move in range(1, tp_n):
+            norm_tokens(piece, lax.rem(spot + move, tp_n) * chunk, chunk)
+
+    inner = jnp.logical_and(fs > 0, fs < fs_n - 1)
+
+    def relay_mixer(some):
+        send_some(some, True)
+        relays(some)
+
+    outer = jnp.logical_not(inner)
+
+    relays(range(0, 2))
+    for piece in range(piece_n):
+        pass_near(0, piece)
+    relays(range(2, 4))
+    send_some(first, False)
+    for piece in range(piece_n):
+        pass_last(0, piece)
+    relays(range(4, last + 1))
+    send_some(second, False)
+    relay(downs[0])
     wait_weight(0)
     wait_weight(1)
-    relay(downs[0])
-    hidden_half(0, ffn.half)
-    relays(downs[1:2])
-    hidden_half(0, 1 - ffn.half)
+    for piece in range(piece_n):
+        wait_puts(0, piece, (4, 6))
+        hidden_piece(0, piece)
+        if piece == 0:
+            relays(downs[1:2])
+            send_some(third, False)
     relays(downs[2:])
     wait_weight(2)
-    project(0, hidden, down_full)
-    relays(first)
-    cross_sums(0)
-    relays(second)
-    add_branch(0, load_tokens, 1, 0.5)
-    relays(third)
-    pass_puts(1)
+    project(0, 0, hidden, down_full)
+    project(0, 1, hidden, down_full)
+    finish_sends(range(first[0]))
+    pl.when(inner)(lambda: relay_mixer(first))
+    cross_sums(0, 0)
+    cross_sums(0, 1)
+    pl.when(inner)(lambda: relay_mixer(second))
+    pl.when(outer)(lambda: relays(first))
+    add_branch(0, 0, load_tokens, 1, 0.5)
+    pl.when(inner)(lambda: relay_mixer(third))
+    add_branch(0, 1, load_tokens, 1, 0.5)
+    pl.when(outer)(lambda: relays(second))
+    pass_near(1, 0)
+    pass_side(1, 0)
     wait_weight(3)
     wait_weight(4)
-    wait_puts(1)
-    mix(mixer.half)
-    mix(1 - mixer.half)
+    pass_last(1, 0)
+    pl.when(outer)(lambda: relays(third))
+    pass_near(1, 1)
+    pass_side(1, 1)
+    wait_puts(1, 0, (2, 4, 5, 6))
+    mix(0)
     wait_weight(5)
-    project(1, mixed, out_full)
-    cross_sums(1)
-    add_branch(1, load_stream(0), 3, 1.0)
-    pass_puts(2)
-    wait_puts(2)
-    hidden_half(2, ffn.half)
-    hidden_half(2, 1 - ffn.half)
-    project(2, hidden, down_full)
-    cross_sums(2)
-    add_branch(2, load_stream(1), 5, 0.5)
-    pass_puts(3)
-    finish_sends()
+    project(1, 0, mixed, out_full)
+    pass_last(1, 1)
+    wait_puts(1, 1, (2, 4, 5, 6))
+    cross_sums(1, 0)
+    mix(1)
+    project(1, 1, mixed, out_full)
+    add_branch(1, 0, load_stream(0), 3, 1.0)
+    cross_sums(1, 1)
+    add_branch(1, 1, load_stream(0), 3, 1.0)
+    pass_side(2, 0)
+    pass_near(2, 0)
+    pass_last(2, 0)
+    pass_side(2, 1)
+    wait_puts(2, 0, (2, 4, 5, 6))
+    hidden_piece(2, 0)
+    pass_near(2, 1)
+    project(2, 0, hidden, down_full)
+    cross_sums(2, 0)
+    pass_last(2, 1)
+    wait_puts(2, 1, (2, 4, 5, 6))
+    hidden_piece(2, 1)
+    project(2, 1, hidden, down_full)
+    add_branch(2, 0, load_stream(1), 5, 0.5)
+    cross_sums(2, 1)
+    pass_side(3, 0)
+    add_branch(2, 1, load_stream(1), 5, 0.5)
+    pass_side(3, 1)
+    finish_sends(range(first[0], len(units)))
     for phase in range(3):
         finish_phase(phase)
         finish_puts(phase)
-    wait_puts(3)
+    for piece in range(piece_n):
+        wait_puts(3, piece, (2, 5))
     copy = pltpu.make_async_copy(normed.at[3, pl.ds(0, count), :], result, last_sem)
     copy.start()
     finish_puts(3)
@@ -1274,8 +1364,8 @@
     hidden_width = small + extra
     channels = mix_u_weight.shape[1] // 2
     columns = math.gcd(fs_n, 4)
-    chunk = count // tp_n
-    pieces = max(1, chunk // PIECE)
+    pieces = count // BLOCK
+    chunk = BLOCK // tp_n
     vmem = pl.BlockSpec(memory_space=pltpu.VMEM)
     hbm = pl.BlockSpec(memory_space=pl.ANY)
     weights = (gate_weight, up_weight, down_weight, mix_u_weight, mix_v_weight, mix_out_weight)
@@ -1297,27 +1387,27 @@
             pltpu.VMEM((4, 2 * count, width), BF16),
             pltpu.VMEM((2 * count, hidden_width), BF16),
             pltpu.VMEM((2 * count, channels), BF16),
-            pltpu.VMEM((2, chunk, width), BF16),
-            pltpu.VMEM((3, 2 * count, width), BF16),
-            pltpu.VMEM((3, 2, count // 2, width), BF16),
-            pltpu.VMEM((3, 2, chunk, width), BF16),
-            pltpu.VMEM((3, 2, chunk, width), BF16),
-            pltpu.VMEM((3, chunk, width), BF16),
-            pltpu.VMEM((3, chunk, width), BF16),
+            pltpu.VMEM((2, count // tp_n, width), BF16),
+            pltpu.VMEM((3, pieces, 2, 2, BLOCK // 2, width), BF16),
+            pltpu.VMEM((3, pieces, 2, BLOCK // 2, width), BF16),
+            pltpu.VMEM((3, pieces, 2, chunk, width), BF16),
+            pltpu.VMEM((3, pieces, 2, chunk, width), BF16),
+            pltpu.VMEM((3, pieces, chunk, width), BF16),
+            pltpu.VMEM((3, pieces, chunk, width), BF16),
             dma((6, 2)),
             dma((unit_n, 4)),
             dma((unit_n, fs_n)),
             dma((unit_n, fs_n)),
             dma((unit_n, max(1, grp_n - 1), fs_n)),
             dma((unit_n, max(1, grp_n - 1), fs_n)),
-            dma((3, 2, columns)),
-            dma((3, 2, columns)),
-            dma((3, 2, columns)),
-            dma((3, 2, columns)),
-            dma((3, columns)),
-            dma((3, columns)),
-            dma((4, 7, pieces)),
-            dma((4, 7, pieces)),
+            dma((3, pieces)),
+            dma((3, pieces, columns)),
+            dma((3, pieces)),
+            dma((3, pieces, 2, columns)),
+            dma((3, pieces)),
+            dma((3, pieces, columns)),
+            dma((4, 8, pieces)),
+            dma((4, 8, pieces)),
             dma(()),
         ],
         compiler_params=pltpu.CompilerParams(
@@ -1352,7 +1442,7 @@
     return (
         tp_n == 4
         and fs_n == 4
-        and count % (4 * PIECE) == 0
+        and count == 2 * BLOCK
         and rows % (32 * grp_n) == 0
         and hidden_width % 128 == 0
         and halves(hidden_width)[0] % (32 * grp_n) == 0

time: 214 us -> 206 us (0.963)
  Pallas kernels: 211 us -> 204 us
    pallas_call x1, Pallas kernels: 211 us -> 204 us  [shared(): pl.pallas_call(functools.partial(shared_kernel, sizes, units), out_shape=...]
where the time goes in v2:
time: 206 us
  Pallas kernels  204 us (99%)
  local copies, waits for them, and re-layouts  2.3 us (1%)
    pallas_call x1, Pallas kernels, shared(): pl.pallas_call(functools.partial(shared_kernel, sizes, units), out_shape=...  204 us

profile of v2, /device:TPU:1, one launch (start us, length us, event | category | flops | bytes accessed | tf_op | source)
XLA Modules:
  0.0 206.2 jit_solution(10879062572638109839)
XLA Ops:
  0.0 203.9 %shard_map.154 = bf16[256,2048]{1,0:T(8,128)(2,1)} custom-call(bf16[256,2048]{1,0:T(8,128)(2,1)} %tokens.1, bf16[2048]{0:T(1024)(128)(2,1)} %gain0.1, bf16[2048]{0:T(1024)(128)(2,1)} %gain1.1, bf16[2048]{0:T(1024)(128)(2,1)} %gain2.1, bf16[2048]{0:T(1024)(128)(2,1)} %gain3.1, bf16[2048]{0:T(1024)(128)(2,1)} %gain4.1, bf16[2048]{0:T(1024)(128)(2,1)} %gain5.1, ...), custom_call_target="tpu_custom_call" | custom-call | tf_op jit(solution)/shard_map/pallas_call | solution.py:1375
  203.9 2.3 %copy.18 = bf16[256,2048]{1,0:T(8,128)(2,1)} copy(bf16[256,2048]{1,0:T(8,128)(2,1)} %shard_map.154) | data formatting | bytes 2097152

commit v3 on v2

--- a/solution.py
+++ b/solution.py
@@ -607,17 +607,20 @@
     )
 
 
-FFN_PAIR = "far"
-MIX_PAIR = "near"
 PIECES = (2, 2, 2, 1, 1, 1)
 AHEAD = 3
 LAG = 2
 ROW_SPLIT = (2, 5)
+END_GROUPS = 1
 
 
 def halves(size):
     small = size // 256 * 128
     return small, size - 2 * small
+
+
+def end_share(size):
+    return size // (4 * GROUP_WIDTH) * END_GROUPS * GROUP_WIDTH
 
 
 def weight_units(shapes, grp_n):
@@ -627,18 +630,24 @@
         for w in group:
             rows, cols = shapes[w]
             split = w in ROW_SPLIT
-            small, extra = halves(rows if split else cols)
-            span = small if split else rows
-            share = span // grp_n
-            piece = share // PIECES[w]
+            size = rows if split else cols
+            small, extra = halves(size)
+            ends = end_share(size)
+            if w < 3:
+                cuts = [("side", (0, small + extra), 0, small, PIECES[w])]
+                if extra:
+                    cuts.append(("middle", (small, small), small, extra, 1))
+            else:
+                cuts = [
+                    ("middle", (ends, ends), 0, size - ends, PIECES[w]),
+                    ("ends", (0, 0), 0, ends, PIECES[w]),
+                ]
             mine = []
-            for n in range(PIECES[w]):
-                width = cols if split else small
-                mine.append((w, n * piece, share, piece, 0, width, False))
-            if extra and split:
-                mine.append((w, small, extra // grp_n, extra // grp_n, 0, cols, True))
-            elif extra:
-                mine.append((w, 0, rows // grp_n, rows // grp_n, small, extra, True))
+            for route, source, target, span, pieces in cuts:
+                share = (span if split else rows) // grp_n
+                piece = share // pieces
+                for n in range(pieces):
+                    mine.append((w, route, source, target, span, share, n * piece, piece))
             made.append(mine)
         for n in range(max(len(mine) for mine in made)):
             units += [mine[n] for mine in made if n < len(mine)]
@@ -710,7 +719,7 @@
     far_spot = core * chips + 1 - chip
     columns = pair_recv.shape[2]
     column = width // columns
-    piece_n = put_send.shape[2]
+    piece_n = put_send.shape[1]
     piece_rows = count // piece_n
     chunk = piece_rows // tp_n
     all_gains = (gain0, gain1, gain2, gain3, gain4, gain5)
@@ -722,23 +731,18 @@
     second = [unit for unit in range(len(units)) if units[unit][0] == 4]
     third = [unit for unit in range(len(units)) if units[unit][0] == 5]
 
+    inner = jnp.logical_and(fs > 0, fs < fs_n - 1)
+    outer = jnp.logical_not(inner)
+
     class Near:
-        half = lax.rem(fs, 2)
+        half = jnp.where(inner, 1, 0)
         partner = fs + 1 - 2 * lax.rem(fs, 2)
-        reach = 2
-        left_ok, right_ok = fs >= 2, fs + 2 < fs_n
-        other_left, other_right = (fs >= 1, fs - 1), (fs + 1 < fs_n, fs + 1)
 
     class Far:
         half = fs // middle
         partner = lax.rem(fs + middle, fs_n)
-        reach = 1
-        left_ok, right_ok = lax.rem(fs, middle) > 0, lax.rem(fs, middle) < middle - 1
-        other_left, other_right = (fs >= middle, middle - 1), (fs < middle, middle)
-
-    named = {"near": Near, "far": Far}
-    ffn, mixer = named[FFN_PAIR], named[MIX_PAIR]
-    pairs = (ffn, ffn, ffn, mixer, mixer, mixer)
+
+    ffn, mixer = Far, Near
     phases = (ffn, mixer, ffn)
 
     barrier = pltpu.get_barrier_semaphore()
@@ -756,50 +760,45 @@
         )
     pl.semaphore_wait(barrier, fs_n - 1 + grp_n - 1 + tp_n - 1)
 
-    def large(half):
-        return (half + core) % 2 == 0
-
-    def half_start(w, half):
-        small, extra = halves(shards[w].shape[0 if w in ROW_SPLIT else 1])
-        return half * (small + extra * (1 - core))
-
     def view(unit, block):
-        w, low, share, rows, col, cols, _ = units[unit]
-        start = low + grp * share
+        w, _, _, target, span, share, low, rows = units[unit]
+        start = grp * share + low
         if w in ROW_SPLIT:
-            return fulls[w].at[block, pl.ds(aligned(start, 16), rows), :]
+            return fulls[w].at[block, pl.ds(aligned(target + start, 16), rows), :]
         start = aligned(block * shards[w].shape[0] + start, 16)
-        return fulls[w].at[pl.ds(start, rows), pl.ds(col, cols)]
+        return fulls[w].at[pl.ds(start, rows), pl.ds(target, span)]
 
     def shard_view(unit, half):
-        w, low, share, rows, col, cols, _ = units[unit]
-        start = low + grp * share
-        base = half_start(w, half)
+        w, _, source, _, span, share, low, rows = units[unit]
+        start = grp * share + low
+        base = source[0] + half * (source[1] - source[0])
         if w in ROW_SPLIT:
             return shards[w].at[pl.ds(aligned(base + start, 16), rows), :]
-        return shards[w].at[pl.ds(aligned(start, 16), rows), pl.ds(aligned(base + col, 128), cols)]
-
-    def has(unit, half):
-        return large(half) if units[unit][6] else True
+        return shards[w].at[pl.ds(aligned(start, 16), rows), pl.ds(aligned(base, 128), span)]
+
+    def has(unit):
+        return {"side": True, "middle": inner, "ends": outer}[units[unit][1]]
 
     def own_copies(w):
-        half = pairs[w].half
-        base = half_start(w, half)
-        small, extra = halves(shards[w].shape[0 if w in ROW_SPLIT else 1])
-
-        def part(low, size, sem):
+        size = shards[w].shape[0 if w in ROW_SPLIT else 1]
+        small, extra = halves(size)
+        ends = end_share(size)
+
+        def part(base, low, span, sem):
             if w in ROW_SPLIT:
-                source = shards[w].at[pl.ds(aligned(base + low, 128), size), :]
-                target = fulls[w].at[fs, pl.ds(low, size), :]
+                source = shards[w].at[pl.ds(aligned(base, 128), span), :]
+                target = fulls[w].at[fs, pl.ds(low, span), :]
             else:
                 rows = shards[w].shape[0]
-                source = shards[w].at[:, pl.ds(aligned(base + low, 128), size)]
-                target = fulls[w].at[pl.ds(aligned(fs * rows, 16), rows), pl.ds(low, size)]
+                source = shards[w].at[:, pl.ds(aligned(base, 128), span)]
+                target = fulls[w].at[pl.ds(aligned(fs * rows, 16), rows), pl.ds(low, span)]
             return pltpu.make_async_copy(source, target, own_sem.at[w, sem])
 
-        made = [(True, part(0, small, 0))]
+        if w >= 3:
+            return [(inner, part(ends, 0, size - ends, 0)), (outer, part(0, 0, ends, 1))]
+        made = [(True, part(ffn.half * (small + extra), 0, small, 0))]
         if extra:
-            made.append((large(half), part(small, extra, 1)))
+            made.append((inner, part(small, small, extra, 1)))
         return made
 
     def guarded(ok, act):
@@ -808,15 +807,9 @@
         else:
             pl.when(ok)(act)
 
-    def both(a, b):
-        if a is True:
-            return b
-        if b is True:
-            return a
-        return a & b
-
     def fresh_copies(unit):
-        pair = pairs[units[unit][0]]
+        route = units[unit][1]
+        half = ffn.half
         block = view(unit, fs)
 
         def made(slot, half, target):
@@ -829,48 +822,71 @@
                 device_id_type=MESH,
             )
 
-        own, other = pair.half, 1 - pair.half
-        near, away = has(unit, own), has(unit, other)
-        left, right = fs - pair.reach, fs + pair.reach
-        other_left, other_right = pair.other_left[1], pair.other_right[1]
+        if route == "middle":
+            return (
+                (fs != middle - 1, lambda: made(0, 0, middle - 1)),
+                (fs != middle, lambda: made(1, 0, middle)),
+            )
+        if route == "ends":
+            return (
+                (fs > 0, lambda: made(0, 0, 0)),
+                (fs < fs_n - 1, lambda: made(1, 0, fs_n - 1)),
+            )
+        near = fs + 1 - 2 * lax.rem(fs, 2)
         return (
-            (both(pair.left_ok, near), left, lambda: made(0, own, left)),
-            (both(pair.right_ok, near), right, lambda: made(1, own, right)),
-            (both(pair.other_left[0], away), other_left, lambda: made(2, other, other_left)),
-            (both(pair.other_right[0], away), other_right, lambda: made(3, other, other_right)),
+            (True, lambda: made(0, half, near)),
+            (True, lambda: made(1, 1 - half, jnp.where(fs < middle, middle, middle - 1))),
         )
 
     def send_own(unit):
         if unit < first[0]:
-            for ok, _, copy in fresh_copies(unit):
+            for ok, copy in fresh_copies(unit):
                 guarded(ok, lambda copy=copy: copy().start())
 
-    def send_some(some, ends):
+    def send_some(some, route):
         for unit in some:
-            for ok, target, copy in fresh_copies(unit):
-                inner = jnp.logical_and(target > 0, target < fs_n - 1)
-                chosen = jnp.logical_not(inner) if ends else inner
-                guarded(jnp.logical_and(ok, chosen), lambda copy=copy: copy().start())
+            if units[unit][1] == route:
+                for ok, copy in fresh_copies(unit):
+                    guarded(ok, lambda copy=copy: copy().start())
 
     def relay_copy(unit, block, leftward):
-        pair = pairs[units[unit][0]]
         target = view(unit, block)
         return pltpu.make_async_remote_copy(
             src_ref=target,
             dst_ref=target,
             send_sem=relay_send.at[unit, block],
             recv_sem=relay_recv.at[unit, block],
-            device_id={"fs": fs - pair.reach if leftward else fs + pair.reach},
+            device_id={"fs": fs - 1 if leftward else fs + 1},
             device_id_type=MESH,
         )
+
+    def goes_on(unit, leftward, act):
+        if units[unit][1] == "side":
+            pl.when(lax.rem(fs, middle) == (1 if leftward else 0))(act)
 
     def side_copy(unit, block, move):
         target = view(unit, block)
         return pltpu.make_async_remote_copy(
             src_ref=target,
             dst_ref=target,
-            send_sem=side_send.at[unit, move - 1, block],
-            recv_sem=side_recv.at[unit, move - 1, block],
+            send_sem=side_send.at[unit, move - 1],
+            recv_sem=side_recv.at[unit, move - 1],
+            device_id={"grp": lax.rem(grp + move, grp_n)},
+            device_id_type=MESH,
+        )
+
+    def side_total(unit, move):
+        w, _, _, target, span, share, low, rows = units[unit]
+        others = fs_n - 1
+        if w in ROW_SPLIT:
+            total = fulls[w].at[pl.ds(0, others), pl.ds(0, rows), :]
+        else:
+            total = fulls[w].at[pl.ds(0, others * rows), pl.ds(target, span)]
+        return pltpu.make_async_remote_copy(
+            src_ref=total,
+            dst_ref=total,
+            send_sem=side_send.at[unit, move - 1],
+            recv_sem=side_recv.at[unit, move - 1],
             device_id={"grp": lax.rem(grp + move, grp_n)},
             device_id_type=MESH,
         )
@@ -890,18 +906,13 @@
 
             lax.fori_loop(1, fs_n, step, 0)
 
-        pair = pairs[units[unit][0]]
-        guarded(has(unit, pair.half), whole)
+        guarded(has(unit), whole)
 
     def relay(unit):
-        pair = pairs[units[unit][0]]
-
         def act(block, leftward):
             relay_copy(unit, block, leftward).wait_recv()
 
-            @pl.when(pair.left_ok if leftward else pair.right_ok)
-            def _():
-                relay_copy(unit, block, leftward).start()
+            goes_on(unit, leftward, lambda: relay_copy(unit, block, leftward).start())
 
             for move in range(1, grp_n):
                 side_copy(unit, block, move).start()
@@ -915,27 +926,26 @@
         for unit in range(len(units)):
             if units[unit][0] == w:
 
-                def act(block, leftward, unit=unit):
+                def act(unit=unit):
                     for move in range(1, grp_n):
-                        side_copy(unit, block, move).wait_recv()
-
-                over_blocks(unit, act)
+                        side_total(unit, move).wait_recv()
+
+                guarded(has(unit), act)
 
     def finish_sends(some):
         for unit in some:
-            pair = pairs[units[unit][0]]
-            for ok, _, copy in fresh_copies(unit):
+            for ok, copy in fresh_copies(unit):
                 guarded(ok, lambda copy=copy: copy().wait_send())
 
-            def act(block, leftward, unit=unit, pair=pair):
-                @pl.when(pair.left_ok if leftward else pair.right_ok)
-                def _():
-                    relay_copy(unit, block, leftward).wait_send()
-
+            def act(block, leftward, unit=unit):
+                goes_on(unit, leftward, lambda: relay_copy(unit, block, leftward).wait_send())
+
+            def sides(unit=unit):
                 for move in range(1, grp_n):
-                    side_copy(unit, block, move).wait_send()
+                    side_total(unit, move).wait_send()
 
             over_blocks(unit, act)
+            guarded(has(unit), sides)
 
     def column_span(col):
         return pl.ds(aligned(col * column, 128), column)
@@ -992,6 +1002,11 @@
         if phase == 3:
             start = piece * piece_rows + inside
         return pl.ds(aligned(start, 16), size)
+
+    def put_slot(phase, which):
+        before = (0, 4, 11, 18)[phase]
+        kinds = ((1, 3, 4, 6), (0, 1, 2, 3, 4, 5, 6), (0, 1, 2, 3, 4, 5, 6), (0, 2, 5))[phase]
+        return before + kinds.index(3 if which == 7 else which)
 
     def put_copy(phase, which, piece):
         half = phases[phase].half if phase < 3 else 0
@@ -1007,8 +1022,8 @@
         return pltpu.make_async_remote_copy(
             src_ref=rows,
             dst_ref=rows,
-            send_sem=put_send.at[phase, which, piece],
-            recv_sem=put_recv.at[phase, which, piece],
+            send_sem=put_send.at[put_slot(phase, which), piece],
+            recv_sem=put_recv.at[put_slot(phase, which), piece],
             device_id=target,
             device_id_type=MESH,
         )
@@ -1186,13 +1201,13 @@
     def mix(piece):
         at = lax.broadcasted_iota(jnp.int32, (BLOCK, BLOCK), 0)
         to = lax.broadcasted_iota(jnp.int32, (BLOCK, BLOCK), 1)
-        half = mixer.half
         here = mixed.shape[1]
         groups = here // GROUP_WIDTH
-        all_gain = spatial_gain[...].astype(F32).reshape(1, 2 * here)
-        all_gain = jnp.where(half == 0, all_gain[:, :here], all_gain[:, here:])
+        shift = spatial_weight.shape[0] - groups
+        all_gain = spatial_gain[...].astype(F32).reshape(1, spatial_gain.shape[0])
+        all_gain = jnp.where(inner, all_gain[:, all_gain.shape[1] - here :], all_gain[:, :here])
         all_bias = spatial_bias[...].astype(F32)
-        all_bias = jnp.where(half == 0, all_bias[:groups], all_bias[groups:])
+        all_bias = jnp.where(inner, all_bias[shift:], all_bias[:groups])
 
         def block(n, carry):
             rows = pl.ds(aligned(piece * 2 * piece_rows + n * BLOCK, 16), BLOCK)
@@ -1205,7 +1220,7 @@
                 v = v - jnp.mean(v, axis=-1, keepdims=True)
                 v = v * lax.rsqrt(jnp.mean(v * v, axis=-1, keepdims=True) + 1e-05)
                 v = (v * all_gain[:, span]).astype(BF16)
-                weight = spatial_weight[half * groups + g].astype(F32)
+                weight = spatial_weight[g + shift * mixer.half].astype(F32)
                 weight = jnp.where(at >= to, weight, 0.0).astype(BF16)
                 bias = jnp.where(at == to, all_bias[g : g + 1, :], 0.0)
                 bias = jnp.sum(bias, axis=1, keepdims=True)
@@ -1235,37 +1250,37 @@
         norm_tokens(piece, spot * chunk, chunk)
         start_puts(0, piece)
 
-    small, extra = halves(gate_w.shape[1])
-    if extra:
-
-        @pl.when(jnp.logical_not(large(ffn.half)))
-        def _():
-            for full in (gate_full, up_full):
-                full[:, pl.ds(small, extra)] = jnp.zeros((full.shape[0], extra), BF16)
-            pad = jnp.zeros((fs_n, extra, down_full.shape[2]), BF16)
-            down_full[:, pl.ds(small, extra), :] = pad
+    def clear(pads, low):
+        for full in pads:
+            size = full.shape[-1] if len(full.shape) == 2 else full.shape[1]
+            if low == size:
+                continue
+            if len(full.shape) == 2:
+                full[:, pl.ds(low, size - low)] = jnp.zeros((full.shape[0], size - low), BF16)
+            else:
+                blank = jnp.zeros((fs_n, size - low, full.shape[2]), BF16)
+                full[:, pl.ds(low, size - low), :] = blank
+
+    @pl.when(outer)
+    def _():
+        small, extra = halves(gate_w.shape[1])
+        if extra:
+            clear((gate_full, up_full, down_full), small)
+        clear((u_full, v_full, out_full), end_share(u_w.shape[1]))
 
     for piece in range(piece_n):
         for move in range(1, tp_n):
             norm_tokens(piece, lax.rem(spot + move, tp_n) * chunk, chunk)
-
-    inner = jnp.logical_and(fs > 0, fs < fs_n - 1)
-
-    def relay_mixer(some):
-        send_some(some, True)
-        relays(some)
-
-    outer = jnp.logical_not(inner)
 
     relays(range(0, 2))
     for piece in range(piece_n):
         pass_near(0, piece)
     relays(range(2, 4))
-    send_some(first, False)
+    send_some(first, "middle")
     for piece in range(piece_n):
         pass_last(0, piece)
     relays(range(4, last + 1))
-    send_some(second, False)
+    send_some(second, "middle")
     relay(downs[0])
     wait_weight(0)
     wait_weight(1)
@@ -1274,19 +1289,23 @@
         hidden_piece(0, piece)
         if piece == 0:
             relays(downs[1:2])
-            send_some(third, False)
+            send_some(third, "middle")
     relays(downs[2:])
+    pl.when(inner)(lambda: relays(first))
     wait_weight(2)
     project(0, 0, hidden, down_full)
     project(0, 1, hidden, down_full)
     finish_sends(range(first[0]))
-    pl.when(inner)(lambda: relay_mixer(first))
+    send_some(first, "ends")
+    pl.when(outer)(lambda: send_some(second + third, "ends"))
+    pl.when(inner)(lambda: relays(second))
     cross_sums(0, 0)
     cross_sums(0, 1)
-    pl.when(inner)(lambda: relay_mixer(second))
+    pl.when(inner)(lambda: send_some(second, "ends"))
+    pl.when(inner)(lambda: relays(third))
     pl.when(outer)(lambda: relays(first))
     add_branch(0, 0, load_tokens, 1, 0.5)
-    pl.when(inner)(lambda: relay_mixer(third))
+    pl.when(inner)(lambda: send_some(third, "ends"))
     add_branch(0, 1, load_tokens, 1, 0.5)
     pl.when(outer)(lambda: relays(second))
     pass_near(1, 0)
@@ -1362,7 +1381,7 @@
     count, width = tokens.shape
     small, extra = halves(gate_weight.shape[1])
     hidden_width = small + extra
-    channels = mix_u_weight.shape[1] // 2
+    channels = mix_u_weight.shape[1] - end_share(mix_u_weight.shape[1])
     columns = math.gcd(fs_n, 4)
     pieces = count // BLOCK
     chunk = BLOCK // tp_n
@@ -1395,19 +1414,19 @@
             pltpu.VMEM((3, pieces, chunk, width), BF16),
             pltpu.VMEM((3, pieces, chunk, width), BF16),
             dma((6, 2)),
-            dma((unit_n, 4)),
+            dma((unit_n, 2)),
             dma((unit_n, fs_n)),
             dma((unit_n, fs_n)),
-            dma((unit_n, max(1, grp_n - 1), fs_n)),
-            dma((unit_n, max(1, grp_n - 1), fs_n)),
+            dma((unit_n, max(1, grp_n - 1))),
+            dma((unit_n, max(1, grp_n - 1))),
             dma((3, pieces)),
             dma((3, pieces, columns)),
             dma((3, pieces)),
             dma((3, pieces, 2, columns)),
             dma((3, pieces)),
             dma((3, pieces, columns)),
-            dma((4, 8, pieces)),
-            dma((4, 8, pieces)),
+            dma((21, pieces)),
+            dma((21, pieces)),
             dma(()),
         ],
         compiler_params=pltpu.CompilerParams(
@@ -1446,7 +1465,7 @@
         and rows % (32 * grp_n) == 0
         and hidden_width % 128 == 0
         and halves(hidden_width)[0] % (32 * grp_n) == 0
-        and channels % (2 * GROUP_WIDTH) == 0
+        and channels % (4 * GROUP_WIDTH) == 0
     )
 
 

time: 206 us -> 200 us (0.971)
  Pallas kernels: 204 us -> 198 us
    pallas_call x1, Pallas kernels: 204 us -> 198 us  [shared(): pl.pallas_call(functools.partial(shared_kernel, sizes, units), out_shape=...]
where the time goes in v3:
time: 200 us
  Pallas kernels  198 us (99%)
  local copies, waits for them, and re-layouts  2.3 us (1%)
    pallas_call x1, Pallas kernels, shared(): pl.pallas_call(functools.partial(shared_kernel, sizes, units), out_shape=...  198 us

profile of v3, /device:TPU:1, one launch (start us, length us, event | category | flops | bytes accessed | tf_op | source)
XLA Modules:
  0.0 199.9 jit_solution(9367273640009691852)
XLA Ops:
  0.0 197.6 %shard_map.154 = bf16[256,2048]{1,0:T(8,128)(2,1)} custom-call(bf16[256,2048]{1,0:T(8,128)(2,1)} %tokens.1, bf16[2048]{0:T(1024)(128)(2,1)} %gain0.1, bf16[2048]{0:T(1024)(128)(2,1)} %gain1.1, bf16[2048]{0:T(1024)(128)(2,1)} %gain2.1, bf16[2048]{0:T(1024)(128)(2,1)} %gain3.1, bf16[2048]{0:T(1024)(128)(2,1)} %gain4.1, bf16[2048]{0:T(1024)(128)(2,1)} %gain5.1, ...), custom_call_target="tpu_custom_call" | custom-call | tf_op jit(solution)/shard_map/pallas_call | solution.py:1394
  197.6 2.3 %copy.18 = bf16[256,2048]{1,0:T(8,128)(2,1)} copy(bf16[256,2048]{1,0:T(8,128)(2,1)} %shard_map.154) | data formatting | bytes 2097152

commit v4 on v3

--- a/solution.py
+++ b/solution.py
@@ -608,7 +608,7 @@
 
 
 PIECES = (2, 2, 2, 1, 1, 1)
-AHEAD = 3
+AHEAD = 4
 LAG = 2
 ROW_SPLIT = (2, 5)
 END_GROUPS = 1
@@ -1272,14 +1272,13 @@
         for move in range(1, tp_n):
             norm_tokens(piece, lax.rem(spot + move, tp_n) * chunk, chunk)
 
-    relays(range(0, 2))
+    relays(range(0, 4))
     for piece in range(piece_n):
         pass_near(0, piece)
-    relays(range(2, 4))
     send_some(first, "middle")
+    relays(range(4, last + 1))
     for piece in range(piece_n):
         pass_last(0, piece)
-    relays(range(4, last + 1))
     send_some(second, "middle")
     relay(downs[0])
     wait_weight(0)

time: 200 us -> 194 us (0.970)
  Pallas kernels: 198 us -> 191 us
    pallas_call x1, Pallas kernels: 198 us -> 191 us  [shared(): pl.pallas_call(functools.partial(shared_kernel, sizes, units), out_shape=...]
where the time goes in v4:
time: 194 us; the launch traced here: 193 us
  Pallas kernels  191 us (98%)
  local copies, waits for them, and re-layouts  2.3 us (1%)
    pallas_call x1, Pallas kernels, shared(): pl.pallas_call(functools.partial(shared_kernel, sizes, units), out_shape=...  191 us

profile of v4, /device:TPU:1, one launch (start us, length us, event | category | flops | bytes accessed | tf_op | source)
XLA Modules:
  0.0 193.4 jit_solution(3479264613909283690)
XLA Ops:
  0.0 191.1 %shard_map.154 = bf16[256,2048]{1,0:T(8,128)(2,1)} custom-call(bf16[256,2048]{1,0:T(8,128)(2,1)} %tokens.1, bf16[2048]{0:T(1024)(128)(2,1)} %gain0.1, bf16[2048]{0:T(1024)(128)(2,1)} %gain1.1, bf16[2048]{0:T(1024)(128)(2,1)} %gain2.1, bf16[2048]{0:T(1024)(128)(2,1)} %gain3.1, bf16[2048]{0:T(1024)(128)(2,1)} %gain4.1, bf16[2048]{0:T(1024)(128)(2,1)} %gain5.1, ...), custom_call_target="tpu_custom_call" | custom-call | tf_op jit(solution)/shard_map/pallas_call | solution.py:1393
  191.1 2.3 %copy.18 = bf16[256,2048]{1,0:T(8,128)(2,1)} copy(bf16[256,2048]{1,0:T(8,128)(2,1)} %shard_map.154) | data formatting | bytes 2097152

commit v5 on v4

--- a/solution.py
+++ b/solution.py
@@ -1302,11 +1302,10 @@
     cross_sums(0, 1)
     pl.when(inner)(lambda: send_some(second, "ends"))
     pl.when(inner)(lambda: relays(third))
-    pl.when(outer)(lambda: relays(first))
     add_branch(0, 0, load_tokens, 1, 0.5)
     pl.when(inner)(lambda: send_some(third, "ends"))
     add_branch(0, 1, load_tokens, 1, 0.5)
-    pl.when(outer)(lambda: relays(second))
+    pl.when(outer)(lambda: relays(first + second))
     pass_near(1, 0)
     pass_side(1, 0)
     wait_weight(3)

time: 194 us -> 195 us (level)
  Pallas kernels: 191 us -> 193 us
where the time goes in v5:
time: 195 us
  Pallas kernels  193 us (99%)
  local copies, waits for them, and re-layouts  2.3 us (1%)
    pallas_call x1, Pallas kernels, shared(): pl.pallas_call(functools.partial(shared_kernel, sizes, units), out_shape=...  193 us

profile of v5, /device:TPU:1, one launch (start us, length us, event | category | flops | bytes accessed | tf_op | source)
XLA Modules:
  0.0 194.9 jit_solution(746559113080964058)
XLA Ops:
  0.0 192.5 %shard_map.154 = bf16[256,2048]{1,0:T(8,128)(2,1)} custom-call(bf16[256,2048]{1,0:T(8,128)(2,1)} %tokens.1, bf16[2048]{0:T(1024)(128)(2,1)} %gain0.1, bf16[2048]{0:T(1024)(128)(2,1)} %gain1.1, bf16[2048]{0:T(1024)(128)(2,1)} %gain2.1, bf16[2048]{0:T(1024)(128)(2,1)} %gain3.1, bf16[2048]{0:T(1024)(128)(2,1)} %gain4.1, bf16[2048]{0:T(1024)(128)(2,1)} %gain5.1, ...), custom_call_target="tpu_custom_call" | custom-call | tf_op jit(solution)/shard_map/pallas_call | solution.py:1392
  192.6 2.3 %copy.18 = bf16[256,2048]{1,0:T(8,128)(2,1)} copy(bf16[256,2048]{1,0:T(8,128)(2,1)} %shard_map.154) | data formatting | bytes 2097152
